TPU v7x, 1024 devices: a whole 4x8x16 slice. The times are simulated.
1024 devices in a mesh: kv: 128 (over z, y), tp: 8 (over x, core).
Axes of the slice: x: 4, y: 8, z: 16, core: 2. Of those that a mesh axis runs over, the one named last changes fastest.
Arguments:
- queries: bfloat16 [16384, 1024], P('kv', 'tp'), may hold values from -6 to 6
- keys: bfloat16 [16384, 512], P('kv', 'tp'), may hold values from -6 to 6
- values: bfloat16 [16384, 512], P('kv', 'tp'), may hold values from -6 to 6
- hidden: bfloat16 [16384, 2048], P('kv'), may hold values from -6 to 6
- log_sums: float32 [2, 16384, 16], P(None, 'kv', 'tp'), may hold values from -1 to 12
- gates: float32 [2, 16384, 16], P(None, 'kv', 'tp'), may hold values from 0.1 to 0.9
- branch_out: bfloat16 [2, 16384, 1024], P(None, 'kv', 'tp'), may hold values from -6 to 6
- cotangent: bfloat16 [16384, 1024], P('kv', 'tp'), may hold values from -6 to 6
- chosen: int32 [128, 8, 48], P(None, 'tp'), may hold values from -1 to 511, as said below
Outputs:
- grad_queries: float32 [16384, 1024], P('kv', 'tp')
- grad_keys: float32 [16384, 512], P('kv', 'tp')
- grad_values: float32 [16384, 512], P('kv', 'tp')
- grad_weight: float32 [2048, 1024], P('kv', 'tp')
Inputs may be any that keep to these rules, and one draw needn't show every extreme that they name: `chosen`: each list holds global block numbers or -1. All live entries of one list name blocks of distinct owners, owner = entry // 4, none later than the list's range; list d holds min(48, d + 1) live entries, and they come first.
All inputs are finite; a program needn't handle non-finite values.
Results may differ from a plain program's by a relative error of at most 0.0055.
Values may be sent and summed in bfloat16 or wider, within the bound.
No kernel may reach another device: no remote copies, remote signals or barrier semaphores. Data moves between devices by JAX's collectives and lax.ppermute only.
A program may use at most 32 MiB of HBM per device.

v0:
```python
import jax
import jax.numpy as jnp
from jax import lax
from jax.sharding import Mesh
from jax.sharding import PartitionSpec as P

DH = 64
BLK = 32
TOPN = 12
SUB = 4
CMP = 32
KV = ("kv_0", "kv_1")


def in_order(blocks, dim):
    blocks = jnp.moveaxis(blocks, 0, dim)
    lengths = blocks.shape
    return blocks.reshape(*lengths[:dim], lengths[dim] * lengths[dim + 1], *lengths[dim + 2 :])


def all_blocks(array, axes, sequence):
    blocks = array[None]
    for k in sequence:
        blocks = lax.all_gather(blocks, axes[k], axis=0, tiled=True)
    current = [lax.axis_size(axes[k]) for k in reversed(sequence)]
    blocks = blocks.reshape(*current, *array.shape)
    turned = sorted(range(len(sequence)), key=lambda place: sequence[len(sequence) - 1 - place])
    return blocks.transpose(*turned, *range(len(sequence), blocks.ndim)).reshape(-1, *array.shape)


def gathered_by_axis(array, axes, sequence, dim):
    return in_order(all_blocks(array, axes, sequence), dim)


def summed_rows(total, axes):
    for axis in axes:
        total = lax.psum_scatter(total, axis, scatter_dimension=0, tiled=True)
    return total


def branch_grads(query_rows, key_rows, value_rows, seen, log_rows, delta_rows, cot_rows, scale):
    wide = jnp.float32
    scores = jnp.einsum("tgre,gme->grtm", query_rows, key_rows, preferred_element_type=wide) * scale
    log_here = jnp.transpose(log_rows, (1, 2, 0))[..., None]
    delta_here = jnp.transpose(delta_rows, (1, 2, 0))[..., None]
    probs = jnp.where(seen[:, None], jnp.exp(scores - log_here), 0.0)
    probs_low = probs.astype(jnp.bfloat16)
    value_grad = jnp.einsum("grtm,tgre->gme", probs_low, cot_rows, preferred_element_type=wide)
    prob_grad = jnp.einsum("tgre,gme->grtm", cot_rows, value_rows, preferred_element_type=wide)
    score_low = (probs * (prob_grad - delta_here)).astype(jnp.bfloat16)
    query_grad = (
        jnp.einsum("grtm,gme->tgre", score_low, key_rows, preferred_element_type=wide) * scale
    )
    key_grad = (
        jnp.einsum("grtm,tgre->gme", score_low, query_rows, preferred_element_type=wide) * scale
    )
    return (query_grad, key_grad, value_grad)


def shards(queries, keys, values, hidden, log_sums, gates, branch_out, cotangent, chosen):
    wide = jnp.float32
    rows_here = queries.shape[0]
    heads = queries.shape[1] // DH
    groups = keys.shape[1] // DH
    group_heads = heads // groups
    per_block = rows_here // BLK
    per_summary = rows_here // CMP
    blocks_all = chosen.shape[0]
    nsel = chosen.shape[2]
    qrows = rows_here // SUB
    scale = DH ** (-0.5)
    grads_each = jax.vmap(branch_grads, in_axes=(0, 0, 0, 0, 0, 0, 0, None))
    place = lax.axis_index(KV)
    position = place * rows_here + jnp.arange(rows_here, dtype=jnp.int32)
    gated = gates[..., None] * cotangent.reshape(rows_here, heads, DH).astype(wide)[None]
    delta_all = jnp.sum(gated * branch_out.reshape(2, rows_here, heads, DH).astype(wide), -1)
    delta_all = delta_all.reshape(2, rows_here, groups, group_heads)
    gated_low = gated.astype(jnp.bfloat16).reshape(2, rows_here, groups, group_heads, DH)
    log_all = log_sums.reshape(2, rows_here, groups, group_heads)
    query_all = queries.reshape(rows_here, groups, group_heads, DH)
    pairs = jnp.concatenate(
        [keys.reshape(rows_here, groups, DH), values.reshape(rows_here, groups, DH)], -1
    )
    means = jnp.mean(pairs.reshape(per_summary, CMP, groups, 2 * DH).astype(wide), 1).astype(
        jnp.bfloat16
    )
    summaries = gathered_by_axis(means, KV, (0, 1), 0)
    summary_count = summaries.shape[0]
    sum_keys = jnp.transpose(summaries[..., :DH], (1, 0, 2))
    sum_values = jnp.transpose(summaries[..., DH:], (1, 0, 2))
    summary_end = jnp.arange(summary_count, dtype=jnp.int32) * CMP + CMP - 1
    summary_seen = (summary_end[None, :] <= position[:, None])[None]
    query_sum, key_sum, value_sum = branch_grads(
        query_all, sum_keys, sum_values, summary_seen, log_all[0], delta_all[0], gated_low[0], scale
    )
    summary_term = jnp.transpose(jnp.concatenate([key_sum, value_sum], -1), (1, 0, 2))
    listing = lax.dynamic_index_in_dim(chosen, place, 0, keepdims=False)
    live = listing >= 0
    safe = jnp.maximum(listing, 0)
    owner = safe // per_block
    group_index = jnp.arange(groups, dtype=jnp.int32)
    hits = (chosen >= 0) & (chosen // per_block == place)
    wanted = jnp.sum(jnp.where(hits, chosen % per_block, 0), -1)
    asked = jnp.any(hits, -1)
    row_target = safe[..., None] * BLK + jnp.arange(BLK, dtype=jnp.int32)
    pair_blocks = pairs.reshape(per_block, BLK, groups, 2 * DH)
    outbound = pair_blocks[wanted, :, group_index[None, :], :]
    arrived = lax.all_to_all(outbound, KV, split_axis=0, concat_axis=0, tiled=True)
    picked = arrived[owner, group_index[:, None]]

    def by_sub(array):
        rest = array.shape[3:]
        moved = array.reshape((groups, SUB, TOPN * BLK) + rest)
        return jnp.swapaxes(moved, 0, 1)

    picked_sub = by_sub(picked)
    picked_keys = picked_sub[..., :DH]
    picked_values = picked_sub[..., DH:]
    live_rows = by_sub(jnp.broadcast_to(live[..., None], (groups, nsel, BLK)))
    key_position = by_sub(row_target)
    sub_position = position.reshape(SUB, qrows)
    block_seen = live_rows[:, :, None, :] & (
        key_position[:, :, None, :] <= sub_position[:, None, :, None]
    )
    query_sel, key_sel, value_sel = grads_each(
        query_all.reshape(SUB, qrows, groups, group_heads, DH),
        picked_keys,
        picked_values,
        block_seen,
        log_all[1].reshape(SUB, qrows, groups, group_heads),
        delta_all[1].reshape(SUB, qrows, groups, group_heads),
        gated_low[1].reshape(SUB, qrows, groups, group_heads, DH),
        scale,
    )
    query_sel = query_sel.reshape(rows_here, groups, group_heads, DH)
    key_sel = jnp.swapaxes(key_sel, 0, 1).reshape(groups, nsel, BLK, DH)
    value_sel = jnp.swapaxes(value_sel, 0, 1).reshape(groups, nsel, BLK, DH)
    slot_grads = jnp.concatenate([key_sel, value_sel], -1)
    slot_grads = slot_grads * live[..., None, None].astype(wide)
    outgoing = (
        jnp.zeros((blocks_all, groups, BLK, 2 * DH), wide)
        .at[owner, group_index[:, None]]
        .add(slot_grads)
    )
    summary_out = jnp.transpose(
        summary_term.reshape(blocks_all, per_summary, groups, 2 * DH), (0, 2, 1, 3)
    )
    both_out = jnp.concatenate([outgoing, summary_out], 2)
    both_in = lax.all_to_all(
        both_out.astype(jnp.bfloat16), KV, split_axis=0, concat_axis=0, tiled=True
    ).astype(both_out.dtype)
    incoming = both_in[:, :, :BLK]
    summary_mine = jnp.transpose(jnp.sum(both_in[:, :, BLK:], 0), (1, 0, 2))
    selector = (
        (wanted[..., None] == jnp.arange(per_block, dtype=jnp.int32)) & asked[..., None]
    ).astype(wide)
    block_sums = jnp.einsum("rgb,rgkc->bkgc", selector, incoming, precision=lax.Precision.HIGHEST)
    pair_grads = (
        block_sums.reshape(rows_here, groups, 2 * DH) + jnp.repeat(summary_mine, CMP, axis=0) / CMP
    )
    grad_queries = (query_sum + query_sel).reshape(rows_here, heads * DH)
    query_low = grad_queries.astype(jnp.bfloat16)
    grad_weight = summed_rows(
        lax.dot_general(
            hidden, query_low, (((0,), (0,)), ((), ())), preferred_element_type=jnp.float32
        ),
        KV,
    )
    grad_keys = pair_grads[..., :DH].reshape(rows_here, groups * DH)
    grad_values = pair_grads[..., DH:].reshape(rows_here, groups * DH)
    return (grad_queries, grad_keys, grad_values, grad_weight)


def solution(mesh):
    finer = Mesh(mesh.devices.reshape(16, 8, mesh.shape["tp"]), ("kv_0", "kv_1", "tp"))
    placed = (
        P(KV, "tp"),
        P(KV, "tp"),
        P(KV, "tp"),
        P(KV, None),
        P(None, KV, "tp"),
        P(None, KV, "tp"),
        P(None, KV, "tp"),
        P(KV, "tp"),
        P(None, "tp", None),
    )
    return jax.shard_map(
        shards,
        mesh=finer,
        in_specs=placed,
        out_specs=(P(KV, "tp"), P(KV, "tp"), P(KV, "tp"), P(KV, "tp")),
        check_vma=False,
    )
```

profile of v0, /device:TPU:6, one launch (start us, length us, event | category | flops | bytes accessed | tf_op | source)
XLA Modules:
  0.0 300.9 jit_solution(4350294956420707934)
XLA Ops:
  7.2 1.3 fusion.53
  8.5 0.8 fusion.41
  9.3 0.5 copy-done.10
  9.8 0.8 copy.104
  10.6 0.8 copy.105
  11.5 0.1 convert_reduce_fusion.1
  11.6 1.7 gather_fusion
  13.3 26.4 %all-to-all-start = ((bf16[128,1,32,128]{3,2,1,0:T(8,128)(2,1)}), bf16[128,1,32,128]{3,2,1,0:T(8,128)(2,1)S(1)}, u32[]{:S(2)}, u32[]{:S(2)}) async-start(bf16[128,1,32,128]{3,2,1,0:T(8,128)(2,1)} %bitcast.35), calls=%async_computation | async-start | bytes 2097152 | tf_op jit(solution)/shard_map/all_to_all | solution.py:108
  39.7 0.1 copy.112
  39.9 0.1 reshape.624
  40.0 0.1 reshape_squeeze.7
  40.1 0.2 convert_reduce_fusion.2
  40.2 0.1 reduce.6
  40.4 0.1 ge.28
  40.5 0.1 broadcast_in_dim.32
  40.5 0.1 broadcast_in_dim.33
  40.6 0.1 add.144
  40.7 0.2 multiply_reduce_fusion
  40.9 0.1 add.141
  41.0 0.1 add.142
  41.1 0.1 copy.114
  41.2 67.7 %all-gather.1 = bf16[16,4,128]{2,1,0:T(4,128)(2,1)S(1)} all-gather(bf16[1,4,128]{2,1,0:T(4,128)(2,1)S(1)} %fusion.49), channel_id=2, replica_groups=mesh['kv_0'=16,'kv_1'=8,'tp'=8] {'kv_0'}, dimensions={0}, use_global_device_ids=true | all-gather | bytes 17408 | tf_op jit(solution)/shard_map/all_gather | solution.py:24
  108.9 25.5 %all_gather.7 = bf16[128,4,1,128]{3,1,2,0:T(4,128)(2,1)S(1)} all-gather(bf16[16,4,1,128]{3,1,2,0:T(4,128)(2,1)S(1)} %bitcast.257), channel_id=1, replica_groups=mesh['kv_0'=16,'kv_1'=8,'tp'=8] {'kv_1'}, dimensions={0}, use_global_device_ids=true | all-gather | bytes 147456 | tf_op jit(solution)/shard_map/all_gather | solution.py:24
  134.4 0.1 copy.110
  134.6 0.1 copy.115
  134.8 0.1 reshape_squeeze.8
  134.9 0.1 copy.122
  135.0 0.1 broadcast_compare_fusion
  135.1 0.3 fusion.54
  135.4 0.3 fusion.15
  135.7 0.2 fusion.19
  135.9 0.1 copy.132
  136.0 0.1 copy.134
  136.2 0.2 fusion.21
  136.4 0.1 copy.135
  136.5 0.2 fusion.44
  136.8 0.1 compare_and_fusion
  136.9 0.7 gather_fusion.1
  137.6 0.3 fusion.13
  137.9 0.3 fusion.26
  138.3 0.4 fusion.16
  138.6 0.7 copy-done.1
  139.3 0.3 fusion.10
  139.6 0.3 copy.128
  139.8 1.2 fusion.24
  141.1 0.2 broadcast.393
  141.3 4.8 %scatter_fusion = f32[128,32,128]{2,1,0:T(8,128)S(1)} fusion(f32[128,32,128]{2,1,0:T(8,128)S(1)} %broadcast.393, s32[48]{0:T(128)S(1)} %get-tuple-element.36, f32[48,32,128]{2,1,0:T(8,128)} %fusion.24), kind=kCustom, calls=%fused_computation.2 | custom fusion | flops 196608 | bytes 2359488 | tf_op jit(solution)/shard_map/scatter-add | solution.py:143
  146.1 0.2 convert_bitcast_fusion
  146.4 1.2 maximum_bitcast_fusion
  147.6 16.0 %all-to-all-start.1 = ((bf16[128,1,36,128]{3,2,1,0:T(8,128)(2,1)}), bf16[128,1,36,128]{3,2,1,0:T(8,128)(2,1)S(1)}, u32[]{:S(2)}, u32[]{:S(2)}) async-start(bf16[128,1,36,128]{3,2,1,0:T(8,128)(2,1)} %maximum_bitcast_fusion), calls=%async_computation.1 | async-start | bytes 2621440 | tf_op jit(solution)/shard_map/all_to_all | solution.py:149
  163.7 0.2 fusion.17
  163.9 0.1 copy.126
  164.0 0.2 fusion.23
  164.2 1.3 convolution_bitcast_fusion
  165.6 0.7 copy.139
  166.3 81.1 %reduce-scatter.5.cloned.1.call-done = f32[128,128]{0,1:T(8,128)} async-done(((f32[2048,128]{0,1:T(8,128)}), f32[128,128]{0,1:T(8,128)}) %reduce-scatter.5.cloned.1.call-update) | async-done | bytes 65552 | tf_op jit(solution)/shard_map/reduce_scatter | solution.py:37
  247.4 1.5 copy.151
  249.0 0.1 slice.80
  249.1 0.4 convolution_bitcast_fusion.6
  249.5 0.1 convert_reduce_fusion
  249.7 0.1 slice_bitcast_fusion.10
  249.8 0.7 copy.141
  250.5 0.7 copy.140
  251.2 42.9 %reduce-scatter.7.cloned.1.call-done = f32[16,128]{1,0:T(8,128)} async-done(((f32[128,128]{1,0:T(8,128)}), f32[16,128]{1,0:T(8,128)}) %reduce-scatter.7.cloned.1.call-update) | async-done | bytes 8208
  (53 shorter events, 0.4 us)
Async XLA Ops:
  7.2 157.0 %copy-start = (bf16[128,2048]{1,0:T(8,128)(2,1)S(1)}, bf16[128,2048]{1,0:T(8,128)(2,1)}, u32[]{:S(2)}) copy-start(bf16[128,2048]{1,0:T(8,128)(2,1)} %param.12) | copy-start | bytes 1572868
  9.3 0.5 copy-start.10
  11.6 28.1 %copy-start.4 = (bf16[128,128]{1,0:T(8,128)(2,1)S(1)}, bf16[128,128]{1,0:T(8,128)(2,1)}, u32[]{:S(2)}) copy-start(bf16[128,128]{1,0:T(8,128)(2,1)} %param.9) | copy-start | bytes 98308
  11.6 28.4 %copy-start.8 = (f32[2,128,2]{1,2,0:T(2,128)S(1)}, f32[2,128,2]{1,2,0:T(2,128)}, u32[]{:S(2)}) copy-start(f32[2,128,2]{1,2,0:T(2,128)} %param.13) | copy-start | bytes 6148
  11.6 28.5 %copy-start.3 = (s32[128,1,48]{0,2,1:T(8,128)S(1)}, s32[128,1,48]{0,2,1:T(8,128)}, u32[]{:S(2)}) copy-start(s32[128,1,48]{0,2,1:T(8,128)} %param.17) | copy-start | bytes 73732
  11.6 29.4 %copy-start.6 = (bf16[128,128]{1,0:T(8,128)(2,1)S(1)}, bf16[128,128]{1,0:T(8,128)(2,1)}, u32[]{:S(2)}) copy-start(bf16[128,128]{1,0:T(8,128)(2,1)} %param.16) | copy-start | bytes 98308
  13.3 121.2 %copy-start.5 = (bf16[2,128,128]{2,1,0:T(8,128)(2,1)S(1)}, bf16[2,128,128]{2,1,0:T(8,128)(2,1)}, u32[]{:S(2)}) copy-start(bf16[2,128,128]{2,1,0:T(8,128)(2,1)} %param.15) | copy-start | bytes 196612
  13.3 121.4 %copy-start.7 = (f32[2,128,2]{1,2,0:T(2,128)S(1)}, f32[2,128,2]{1,2,0:T(2,128)}, u32[]{:S(2)}) copy-start(f32[2,128,2]{1,2,0:T(2,128)} %param.14) | copy-start | bytes 6148
  13.3 123.6 %all-to-all-start = ((bf16[128,1,32,128]{3,2,1,0:T(8,128)(2,1)}), bf16[128,1,32,128]{3,2,1,0:T(8,128)(2,1)S(1)}, u32[]{:S(2)}, u32[]{:S(2)}) async-start(bf16[128,1,32,128]{3,2,1,0:T(8,128)(2,1)} %bitcast.35), calls=%async_computation | async-start | bytes 2097152 | tf_op jit(solution)/shard_map/all_to_all | solution.py:108
  138.6 0.7 copy-start.1
  146.4 17.3 %copy-start.2 = (bf16[4,2,32,384]{3,2,1,0:T(8,128)(2,1)S(1)}, bf16[4,2,32,384]{3,2,1,0:T(8,128)(2,1)}, u32[]{:S(2)}) copy-start(bf16[4,2,32,384]{3,2,1,0:T(8,128)(2,1)} %copy-done.1) | copy-start | bytes 589828
  147.6 101.4 %all-to-all-start.1 = ((bf16[128,1,36,128]{3,2,1,0:T(8,128)(2,1)}), bf16[128,1,36,128]{3,2,1,0:T(8,128)(2,1)S(1)}, u32[]{:S(2)}, u32[]{:S(2)}) async-start(bf16[128,1,36,128]{3,2,1,0:T(8,128)(2,1)} %maximum_bitcast_fusion), calls=%async_computation.1 | async-start | bytes 2621440 | tf_op jit(solution)/shard_map/all_to_all | solution.py:149
  163.6 83.8 %reduce-scatter.5.cloned.1.call-start = ((), (), s32[]{:S(2)}) async-start(), calls=%async_computation.4 | async-start | bytes 1114112 | tf_op jit(solution)/shard_map/reduce_scatter | solution.py:37
  165.5 83.6 %copy-start.9 = (pred[128]{0:T(512)(128)(4,1)S(1)}, pred[128]{0:T(512)(128)(4,1)}, u32[]{:S(2)}) copy-start(pred[128]{0:T(512)(128)(4,1)} %get-tuple-element.22) | copy-start | bytes 388
  165.5 83.6 %copy-start.11 = (s32[128]{0:T(128)S(1)}, s32[128]{0:T(128)}, u32[]{:S(2)}) copy-start(s32[128]{0:T(128)} %copy-done.10) | copy-start | bytes 1540
  165.5 128.6 %reduce-scatter.7.cloned.1.call-start = ((), (), s32[]{:S(2)}) async-start(), calls=%async_computation.5 | async-start | bytes 73728
Sparse Core Ops, SparseCore 0:
  167.8 79.5 reduce-scatter.4
  251.4 42.6 reduce-scatter.6
where the time goes:
time: 302 us; the launch traced here: 301 us
  waiting for transfers between devices  124 us (41%)
  blocking collectives  93.2 us (31%)
  starting transfers between devices  42.5 us (14%)
  between operations  14.5 us (5%)
  local copies, waits for them, and re-layouts  11.5 us (4%)
  other arithmetic  10.9 us (4%)
  matrix products  4.3 us (1%)
    all_gather x2, blocking collectives, all_blocks(): blocks = lax.all_gather(blocks, axes[k], axis=0, tiled=True)  93.2 us
    reduce_scatter x1, waiting for transfers between devices, summed_rows(): total = lax.psum_scatter(total, axis, scatter_dimension=0, tiled=True)  81.1 us
    unnamed x3, waiting for transfers between devices  43 us
    all_to_all x1, starting transfers between devices, shards(): lax.all_to_all(outbound, KV, split_axis=0, concat_axis=0, tiled=True)  26.4 us
    all_to_all x1, starting transfers between devices, shards(): lax.all_to_all(both_out.astype(jnp.bfloat16), KV, split_axis=0, concat_ax...  16 us
    unnamed x32, local copies, waits for them, and re-layouts  6.79 us
  transfers between devices with their start and end apart: 4, of which 2 were waited for; matrix products, arithmetic and copies ran while one was open for 3% of the time, Pallas kernels for 0%

commit v1 on v0

v1 whole, which is shorter than its diff:
```python
import jax
import jax.numpy as jnp
from jax import lax
from jax.experimental import pallas as pl
from jax.experimental.pallas import tpu as pltpu
from jax.sharding import Mesh
from jax.sharding import PartitionSpec as P

DH = 64
BLK = 32
TOPN = 12
SUB = 4
CMP = 32
KV = ("kv_0", "kv_1")
FAR = 1 << 30
WIDE = jnp.float32
LOW = jnp.bfloat16
ROWS = 40


def dot(a, b, ca, cb):
    return lax.dot_general(a, b, (((ca,), (cb,)), ((), ())), preferred_element_type=WIDE)


def outbound_kernel(wanted_ref, keys_ref, values_ref, out_ref, pairs_ref):
    pairs = jnp.concatenate([keys_ref[...], values_ref[...]], -1).astype(WIDE)
    pairs_ref[...] = pairs.astype(LOW).reshape(pairs_ref.shape)
    blocks = pairs_ref.shape[0]
    means = jnp.mean(pairs.reshape(blocks, CMP, 2 * DH), 1)
    tail = jnp.concatenate([means, jnp.zeros((ROWS - BLK - blocks, 2 * DH), WIDE)], 0).astype(LOW)

    def one(d, carry):
        out_ref[d, :BLK, :] = pairs_ref[wanted_ref[d]]
        out_ref[d, BLK:, :] = tail
        return carry

    lax.fori_loop(0, out_ref.shape[0], one, 0, unroll=8)


def main_kernel(own_ref, msum_ref, msel_ref, ldsum_ref, ldsel_ref, relsum_ref, relsel_ref, arr_ref,
                dq_ref, ret_ref, kv_ref):
    rows = dq_ref.shape[0]
    owners = arr_ref.shape[0]
    wide = ROWS - BLK
    scale = DH ** (-0.5)
    both = 2 * rows

    def grads(m, kv, seen, ld):
        half = m.shape[0] // 2
        sd = dot(m, kv, 1, 1)
        probs = jnp.where(seen, jnp.exp(sd[:half] - ld[:, :1]), 0.0)
        ds = (probs * (sd[half:] - ld[:, 1:2])).astype(LOW)
        weights = jnp.concatenate([ds, probs.astype(LOW)], 0)
        return dot(ds, kv, 1, 0), dot(weights, m, 0, 0)

    m = msum_ref[...]
    ld = ldsum_ref[...]
    row_at = lax.broadcasted_iota(jnp.int32, (both, 1), 0) & (rows - 1)
    step = 32
    dq_sum = jnp.zeros((both, 2 * DH), WIDE)
    for first in range(0, owners, step):
        kv = arr_ref[first:first + step, BLK:, :].astype(WIDE).reshape(step * wide, 2 * DH).astype(LOW)
        seen = relsum_ref[:, first * wide:(first + step) * wide] <= row_at
        dq_part, kv_grad = grads(m, kv, seen, ld)
        dq_sum += dq_part
        ret_ref[first:first + step, BLK:, :] = kv_grad.reshape(step, wide, 2 * DH).astype(LOW)
    sub_rows = rows // SUB
    sub_at = lax.broadcasted_iota(jnp.int32, (2 * sub_rows, 1), 0) & (sub_rows - 1)
    for s in range(SUB):
        for i in range(TOPN):
            owner = jnp.maximum(own_ref[s * TOPN + i], 0)
            kv_ref[i * BLK:(i + 1) * BLK, :] = arr_ref[owner, :BLK, :]
        kv = kv_ref[...]
        seen = relsel_ref[s:s + 1, :] <= sub_at + s * sub_rows
        dq_part, kv_grad = grads(msel_ref[s], kv, seen, ldsel_ref[s])
        low = kv_grad.astype(LOW)
        for i in range(TOPN):
            owner = own_ref[s * TOPN + i]

            @pl.when(owner >= 0)
            def _(owner=owner, i=i):
                ret_ref[owner, :BLK, :] = low[i * BLK:(i + 1) * BLK]

        at = s * sub_rows
        for h in range(2):
            total = dq_sum[h * rows + at:h * rows + at + sub_rows, :DH]
            total = total + dq_part[h * sub_rows:(h + 1) * sub_rows, :DH]
            dq_ref[at:at + sub_rows, h * DH:(h + 1) * DH] = total * scale


def weight_kernel(hidden_ref, dq_ref, out_ref):
    low = dq_ref[...].astype(LOW)
    fast, per_slow, cols = out_ref.shape
    slow = hidden_ref.shape[1] // (fast * 16)
    span = fast * 16
    for z in range(slow):
        part = dot(hidden_ref[:, z * span:(z + 1) * span], low, 0, 0).astype(LOW)
        for y in range(fast):
            out_ref[y, z * 16:(z + 1) * 16, :] = part[y * 16:(y + 1) * 16]


def inbound_kernel(chosen_ref, in_ref, gk_ref, gv_ref):
    per_block = gk_ref.shape[0] // BLK

    def one(d, carry):
        sums, tail = carry
        here = in_ref[d, :BLK, :].astype(WIDE)
        pick = chosen_ref[d]
        sums = tuple(sums[b] + jnp.where(pick == b, here, 0.0) for b in range(per_block))
        return sums, tail + in_ref[d, BLK:, :].astype(WIDE)

    zero = jnp.zeros((BLK, 2 * DH), WIDE)
    start = ((zero,) * per_block, jnp.zeros((ROWS - BLK, 2 * DH), WIDE))
    sums, tail = lax.fori_loop(0, in_ref.shape[0], one, start, unroll=4)
    for b in range(per_block):
        total = sums[b] + tail[b:b + 1] * (1.0 / CMP)
        gk_ref[b * BLK:(b + 1) * BLK, :] = total[:, :DH]
        gv_ref[b * BLK:(b + 1) * BLK, :] = total[:, DH:]


def vmem():
    return pl.BlockSpec(memory_space=pltpu.VMEM)


def smem():
    return pl.BlockSpec(memory_space=pltpu.SMEM)


def shards(queries, keys, values, hidden, log_sums, gates, branch_out, cotangent, chosen):
    rows = queries.shape[0]
    heads = queries.shape[1] // DH
    per_block = rows // BLK
    owners = chosen.shape[0]
    nsel = chosen.shape[2]
    sub_rows = rows // SUB
    slow = lax.axis_size(KV[0])
    fast = lax.axis_size(KV[1])
    place = lax.axis_index(KV)
    lists = chosen[:, 0]
    hits = (lists >= 0) & (lists // per_block == place)
    wanted = jnp.sum(jnp.where(hits, lists % per_block, 0), -1)
    asked = jnp.any(hits, -1)
    outbound = pl.pallas_call(
        outbound_kernel,
        out_shape=jax.ShapeDtypeStruct((owners, ROWS, 2 * DH), LOW),
        in_specs=[smem(), vmem(), vmem()],
        out_specs=vmem(),
        scratch_shapes=[pltpu.VMEM((per_block, BLK, 2 * DH), LOW)],
        name="outbound",
    )(wanted, keys, values)
    arrived = lax.all_to_all(outbound, KV, split_axis=0, concat_axis=0, tiled=True)

    gated = gates[..., None] * cotangent.reshape(rows, heads, DH).astype(WIDE)[None]
    delta = jnp.sum(gated * branch_out.reshape(2, rows, heads, DH).astype(WIDE), -1)
    ld = jnp.stack([log_sums, delta], -1)
    gated_low = gated.astype(LOW)
    zero = jnp.zeros((rows, heads, DH), LOW)
    q_part = jnp.concatenate([queries.reshape(rows, heads, DH) * LOW(DH ** (-0.5)), zero], -1)
    g_part = [jnp.concatenate([zero, gated_low[b]], -1) for b in range(2)]
    m_sum = jnp.transpose(jnp.stack([q_part, g_part[0]]), (0, 2, 1, 3)).reshape(-1, 2 * DH)
    m_sel = jnp.stack([q_part, g_part[1]]).reshape(2, SUB, sub_rows, heads, 2 * DH)
    m_sel = jnp.transpose(m_sel, (1, 0, 3, 2, 4)).reshape(SUB, -1, 2 * DH)
    ld_sum = jnp.transpose(ld[0], (1, 0, 2)).reshape(-1, 2)
    ld_sel = jnp.transpose(ld[1].reshape(SUB, sub_rows, heads, 2), (0, 2, 1, 3)).reshape(SUB, -1, 2)
    listing = lax.dynamic_index_in_dim(lists, place, 0, keepdims=False)
    live = listing >= 0
    own = jnp.where(live, listing // per_block, -1)
    starts = jnp.where(live, listing * BLK - place * rows, FAR)
    rel_sel = (starts[:, None] + jnp.arange(BLK, dtype=jnp.int32)).reshape(SUB, TOPN * BLK)
    slot = jnp.arange(owners * (ROWS - BLK), dtype=jnp.int32)
    inner = slot % (ROWS - BLK)
    ends = (slot // (ROWS - BLK) * per_block + inner + 1) * CMP - 1 - place * rows
    rel_sum = jnp.where(inner < per_block, ends, FAR)[None]

    grad_queries, returned = pl.pallas_call(
        main_kernel,
        out_shape=(
            jax.ShapeDtypeStruct((rows, heads * DH), WIDE),
            jax.ShapeDtypeStruct((owners, ROWS, 2 * DH), LOW),
        ),
        in_specs=[smem()] + [vmem()] * 7,
        out_specs=(vmem(), vmem()),
        scratch_shapes=[pltpu.VMEM((TOPN * BLK, 2 * DH), LOW)],
        name="main",
    )(own, m_sum, m_sel, ld_sum, ld_sel, rel_sum, rel_sel, arrived)
    incoming = lax.all_to_all(returned, KV, split_axis=0, concat_axis=0, tiled=True)

    parts = pl.pallas_call(
        weight_kernel,
        out_shape=jax.ShapeDtypeStruct((fast, hidden.shape[1] // fast, heads * DH), LOW),
        in_specs=[vmem(), vmem()],
        out_specs=vmem(),
        name="weight",
    )(hidden, grad_queries)
    across = lax.all_to_all(parts, KV[1], split_axis=0, concat_axis=0, tiled=True)
    column = jnp.sum(across.astype(WIDE), 0).astype(LOW).reshape(slow, -1, heads * DH)
    along = lax.all_to_all(column, KV[0], split_axis=0, concat_axis=0, tiled=True)
    grad_weight = jnp.sum(along.astype(WIDE), 0)

    grad_keys, grad_values = pl.pallas_call(
        inbound_kernel,
        out_shape=(jax.ShapeDtypeStruct((rows, DH), WIDE), jax.ShapeDtypeStruct((rows, DH), WIDE)),
        in_specs=[smem(), vmem()],
        out_specs=(vmem(), vmem()),
        name="inbound",
    )(jnp.where(asked, wanted, per_block), incoming)
    return (grad_queries, grad_keys, grad_values, grad_weight)


def solution(mesh):
    finer = Mesh(mesh.devices.reshape(16, 8, mesh.shape["tp"]), ("kv_0", "kv_1", "tp"))
    placed = (
        P(KV, "tp"),
        P(KV, "tp"),
        P(KV, "tp"),
        P(KV, None),
        P(None, KV, "tp"),
        P(None, KV, "tp"),
        P(None, KV, "tp"),
        P(KV, "tp"),
        P(None, "tp", None),
    )
    return jax.shard_map(
        shards,
        mesh=finer,
        in_specs=placed,
        out_specs=(P(KV, "tp"), P(KV, "tp"), P(KV, "tp"), P(KV, "tp")),
        check_vma=False,
    )
```

time: 302 us -> 227 us (0.75)
  blocking collectives: 93.2 us -> 41 us
  between operations: 14.5 us -> 0.84 us
  Pallas kernels: 0 us -> 13.6 us
  starting transfers between devices: 42.5 us -> 32.7 us
  other arithmetic: 10.9 us -> 5.27 us
  waiting for transfers between devices: 124 us -> 119 us
  matrix products: 4.3 us -> 0 us
    all_gather x2 -> x0, blocking collectives: 93.2 us -> none  [all_blocks(): blocks = lax.all_gather(blocks, axes[k], axis=0, tiled=True)]
    reduce_scatter x1 -> x0, waiting for transfers between devices: 81.1 us -> none  [summed_rows(): total = lax.psum_scatter(total, axis, scatter_dimension=0, tiled=True)]
    all_to_all x1, waiting for transfers between devices: 0.01 us -> 60.7 us  [shards(): lax.all_to_all(returned, KV, split_axis=0, concat_axis=0, tiled=True)]
    all_to_all x1, waiting for transfers between devices: 0.01 us -> 58 us  [shards(): lax.all_to_all(outbound, KV, split_axis=0, concat_axis=0, tiled=True)]
    unnamed x3 -> x0, waiting for transfers between devices: 43 us -> none
    all_to_all x0 -> x2, blocking collectives: none -> 41 us  [the longest x1 21.9 us: shards(): lax.all_to_all(parts, KV[1], split_axis=0, concat_axis=0, tiled=True)]
    pallas_call x0 -> x4, Pallas kernels: none -> 13.6 us  [the longest x1 6.21 us: shards(): pl.pallas_call(main_kernel, out_shape=(jax.ShapeDtypeStruct((rows, heads...]
    all_to_all x1, starting transfers between devices: 16 us -> 6.33 us  [shards(): lax.all_to_all(returned, KV, split_axis=0, concat_axis=0, tiled=True)]
  transfers between devices with their start and end apart: 4 -> 2, of which waited for: 2 -> 2; matrix products, arithmetic and copies ran while one was open for 3% -> 3% of each run, Pallas kernels for 0% -> 0%
where the time goes in v1:
time: 227 us; the launch traced here: 224 us
  waiting for transfers between devices  119 us (52%)
  blocking collectives  41 us (18%)
  starting transfers between devices  32.7 us (14%)
  Pallas kernels  13.6 us (6%)
  local copies, waits for them, and re-layouts  12.3 us (5%)
  other arithmetic  5.27 us (2%)
    all_to_all x1, waiting for transfers between devices, shards(): lax.all_to_all(returned, KV, split_axis=0, concat_axis=0, tiled=True)  60.7 us
    all_to_all x1, waiting for transfers between devices, shards(): lax.all_to_all(outbound, KV, split_axis=0, concat_axis=0, tiled=True)  58 us
    all_to_all x1, starting transfers between devices, shards(): lax.all_to_all(outbound, KV, split_axis=0, concat_axis=0, tiled=True)  26.4 us
    all_to_all x1, blocking collectives, shards(): lax.all_to_all(parts, KV[1], split_axis=0, concat_axis=0, tiled=True)  21.9 us
    all_to_all x1, blocking collectives, shards(): lax.all_to_all(column, KV[0], split_axis=0, concat_axis=0, tiled=True)  19 us
    unnamed x27, local copies, waits for them, and re-layouts  8.72 us
    all_to_all x1, starting transfers between devices, shards(): lax.all_to_all(returned, KV, split_axis=0, concat_axis=0, tiled=True)  6.33 us
    pallas_call x1, Pallas kernels, shards(): pl.pallas_call(main_kernel, out_shape=(jax.ShapeDtypeStruct((rows, heads...  6.21 us
  transfers between devices with their start and end apart: 2, of which 2 were waited for; matrix products, arithmetic and copies ran while one was open for 3% of the time, Pallas kernels for 0%

profile of v1, /device:TPU:6, one launch (start us, length us, event | category | flops | bytes accessed | tf_op | source)
XLA Modules:
  0.0 224.4 jit_solution(2355356671023668198)
XLA Ops:
  0.6 0.8 fusion.12
  1.4 1.3 fusion.3.wanted_ref
  2.7 1.4 copy.44.keys_ref
  4.1 1.4 copy.45.values_ref
  5.6 2.2 outbound.1
  7.7 0.0 copy-start.2
  7.7 0.0 copy-start.4
  7.7 0.0 copy-start.5
  7.7 0.0 copy-start.3
  7.7 0.0 copy-start.7
  7.8 0.0 copy-start.8
  7.8 26.4 %all-to-all-start = ((bf16[128,40,128]{2,1,0:T(8,128)(2,1)}), bf16[128,40,128]{2,1,0:T(8,128)(2,1)S(1)}, u32[]{:S(2)}, u32[]{:S(2)}) async-start(bf16[128,40,128]{2,1,0:T(8,128)(2,1)} %outbound.1), calls=%async_computation | async-start | bytes 2621440 | tf_op jit(solution)/shard_map/all_to_all | solution.py:151
  34.2 0.0 copy-done.2
  34.2 0.2 select_reduce_fusion
  34.4 0.1 select_n.88
  34.5 0.1 add.100
  34.5 0.1 add.97
  34.6 0.1 add.98
  34.7 0.0 copy-done.4
  34.7 0.1 copy.35
  34.8 0.0 copy-done.5
  34.8 0.1 copy.36
  35.0 0.1 copy.49
  35.1 0.0 copy-done.3
  35.1 0.1 copy.41
  35.2 0.0 copy-done.7
  35.3 0.0 copy-done.8
  35.3 0.1 reshape_squeeze.3
  35.4 0.1 copy.48
  35.6 0.1 concatenate.12.clone
  35.7 0.7 copy.40
  36.4 0.8 copy.37
  37.1 0.8 copy.43
  37.9 0.8 copy.42
  38.7 0.6 compare_select_fusion.relsum_ref
  39.3 0.5 compare_select_fusion.1.own_ref
  39.9 0.6 broadcast_add_fusion.relsel_ref
  40.5 58.0 %all-to-all-done.arr_ref = bf16[128,40,128]{2,1,0:T(8,128)(2,1)S(1)} async-done(((bf16[128,40,128]{2,1,0:T(8,128)(2,1)}), bf16[128,40,128]{2,1,0:T(8,128)(2,1)S(1)}, u32[]{:S(2)}, u32[]{:S(2)}) %all-to-all-start) | async-done | bytes 1310752 | tf_op jit(solution)/shard_map/all_to_all | solution.py:151
  98.5 0.0 copy-start
  98.5 1.1 copy-done
  99.6 6.2 %main.1 = (f32[128,128]{1,0:T(8,128)}, bf16[128,40,128]{2,1,0:T(8,128)(2,1)}) custom-call(s32[48]{0:T(128)} %compare_select_fusion.1.own_ref, bf16[512,128]{1,0:T(8,128)(2,1)} %bitcast.69, bf16[4,128,128]{2,1,0:T(8,128)(2,1)} %bitcast.68, f32[256,2]{1,0:T(8,128)} %bitcast.71, f32[4,64,2]{2,1,0:T(8,128)} %bitcast.70, ...), custom_call_target="tpu_custom_call" | custom-call | tf_op jit(solution)/shard_map/main/pallas_call | solution.py:175
  105.8 2.2 weight.1
  108.0 21.9 %all_to_all.20 = bf16[8,256,128]{2,1,0:T(8,128)(2,1)S(1)} all-to-all(bf16[8,256,128]{2,1,0:T(8,128)(2,1)} %weight.1), channel_id=1, replica_groups=mesh['kv_0'=16,'kv_1'=8,'tp'=8] {'kv_1'}, dimensions={0} | all-to-all | bytes 1048576 | tf_op jit(solution)/shard_map/all_to_all | solution.py:195
  129.9 0.1 reduce_sum.41
  130.0 19.0 %all_to_all.21 = bf16[16,16,128]{2,1,0:T(8,128)(2,1)S(1)} all-to-all(bf16[16,16,128]{2,1,0:T(8,128)(2,1)S(1)} %bitcast.76), channel_id=1, replica_groups=mesh['kv_0'=16,'kv_1'=8,'tp'=8] {'kv_0'}, dimensions={0} | all-to-all | bytes 131072 | tf_op jit(solution)/shard_map/all_to_all | solution.py:197
  149.0 0.0 copy-start.6
  149.0 6.3 %all-to-all-start.1 = ((bf16[128,40,128]{2,1,0:T(8,128)(2,1)}), bf16[128,40,128]{2,1,0:T(8,128)(2,1)S(1)}, u32[]{:S(2)}, u32[]{:S(2)}) async-start(bf16[128,40,128]{2,1,0:T(8,128)(2,1)} %get-tuple-element.9), calls=%async_computation.1 | async-start | bytes 2621440 | tf_op jit(solution)/shard_map/all_to_all | solution.py:186
  155.4 0.0 copy-done.6
  155.4 0.5 broadcast_select_fusion.chosen_ref
  155.9 0.6 convert_reduce_fusion
  156.5 60.7 %all-to-all-done.1.in_ref = bf16[128,40,128]{2,1,0:T(8,128)(2,1)S(1)} async-done(((bf16[128,40,128]{2,1,0:T(8,128)(2,1)}), bf16[128,40,128]{2,1,0:T(8,128)(2,1)S(1)}, u32[]{:S(2)}, u32[]{:S(2)}) %all-to-all-start.1) | async-done | bytes 1310752 | tf_op jit(solution)/shard_map/all_to_all | solution.py:186
  217.2 0.0 copy-start.1
  217.2 1.1 copy-done.1
  218.3 3.0 %inbound.1 = (f32[128,64]{1,0:T(8,128)}, f32[128,64]{1,0:T(8,128)}) custom-call(s32[128]{0:T(128)} %broadcast_select_fusion.chosen_ref, bf16[128,40,128]{2,1,0:T(8,128)(2,1)} %copy-done.1), custom_call_target="tpu_custom_call" | custom-call | tf_op jit(solution)/shard_map/inbound/pallas_call | solution.py:200
  221.3 1.5 copy.46
  222.8 1.5 copy.47
  (10 shorter events, 0.1 us)
Async XLA Ops:
  7.7 26.4 %copy-start.2 = (s32[128,1,48]{0,2,1:T(8,128)S(1)}, s32[128,1,48]{0,2,1:T(8,128)}, u32[]{:S(2)}) copy-start(s32[128,1,48]{0,2,1:T(8,128)} %param.17) | copy-start | bytes 73732
  7.7 27.0 %copy-start.4 = (bf16[128,128]{1,0:T(8,128)(2,1)S(1)}, bf16[128,128]{1,0:T(8,128)(2,1)}, u32[]{:S(2)}) copy-start(bf16[128,128]{1,0:T(8,128)(2,1)} %param.9) | copy-start | bytes 98308
  7.7 27.1 %copy-start.5 = (bf16[128,128]{1,0:T(8,128)(2,1)S(1)}, bf16[128,128]{1,0:T(8,128)(2,1)}, u32[]{:S(2)}) copy-start(bf16[128,128]{1,0:T(8,128)(2,1)} %param.16) | copy-start | bytes 98308
  7.7 27.4 %copy-start.3 = (bf16[2,128,128]{2,1,0:T(8,128)(2,1)S(1)}, bf16[2,128,128]{2,1,0:T(8,128)(2,1)}, u32[]{:S(2)}) copy-start(bf16[2,128,128]{2,1,0:T(8,128)(2,1)} %param.15) | copy-start | bytes 196612
  7.7 27.5 %copy-start.7 = (f32[2,128,2]{1,2,0:T(2,128)S(1)}, f32[2,128,2]{1,2,0:T(2,128)}, u32[]{:S(2)}) copy-start(f32[2,128,2]{1,2,0:T(2,128)} %param.14) | copy-start | bytes 6148
  7.8 27.5 %copy-start.8 = (f32[2,128,2]{1,2,0:T(2,128)S(1)}, f32[2,128,2]{1,2,0:T(2,128)}, u32[]{:S(2)}) copy-start(f32[2,128,2]{1,2,0:T(2,128)} %param.13) | copy-start | bytes 6148
  7.8 90.7 %all-to-all-start = ((bf16[128,40,128]{2,1,0:T(8,128)(2,1)}), bf16[128,40,128]{2,1,0:T(8,128)(2,1)S(1)}, u32[]{:S(2)}, u32[]{:S(2)}) async-start(bf16[128,40,128]{2,1,0:T(8,128)(2,1)} %outbound.1), calls=%async_computation | async-start | bytes 2621440 | tf_op jit(solution)/shard_map/all_to_all | solution.py:151
  98.5 1.1 copy-start
  149.0 6.3 %copy-start.6 = (s32[128]{0:T(128)S(1)}, s32[128]{0:T(128)}, u32[]{:S(2)}) copy-start(s32[128]{0:T(128)} %fusion.3.wanted_ref) | copy-start | bytes 1540
  149.0 68.2 %all-to-all-start.1 = ((bf16[128,40,128]{2,1,0:T(8,128)(2,1)}), bf16[128,40,128]{2,1,0:T(8,128)(2,1)S(1)}, u32[]{:S(2)}, u32[]{:S(2)}) async-start(bf16[128,40,128]{2,1,0:T(8,128)(2,1)} %get-tuple-element.9), calls=%async_computation.1 | async-start | bytes 2621440 | tf_op jit(solution)/shard_map/all_to_all | solution.py:186
  217.2 1.1 copy-start.1

commit v2 on v1

v2 whole, which is shorter than its diff:
```python
import jax
import jax.numpy as jnp
from jax import lax
from jax.experimental import pallas as pl
from jax.experimental.pallas import tpu as pltpu
from jax.sharding import Mesh
from jax.sharding import PartitionSpec as P

DH = 64
BLK = 32
TOPN = 12
SUB = 4
CMP = 32
KV = ("kv_0", "kv_1")
FAR = 1 << 30
WIDE = jnp.float32
LOW = jnp.bfloat16
SLOW = 16
FAST = 8
PER = 4
PAIR = 2 * DH
ROWS = PER * BLK
SUB_ROWS = ROWS // SUB
COLS = 16
FETCH = SLOW * (BLK + PER)
SUMS = SLOW * BLK
PARTS = SLOW * (BLK + PER)
BACK = PARTS + SLOW * COLS
LAST = ROWS + 8 + COLS


def dot(a, b, ca, cb):
    return lax.dot_general(a, b, (((ca,), (cb,)), ((), ())), preferred_element_type=WIDE)


def pairs_kernel(keys_ref, values_ref, out_ref):
    both = jnp.concatenate([keys_ref[...], values_ref[...]], 0).astype(WIDE)
    out_ref[...] = both.T.astype(LOW)


def relay_kernel(table_ref, all_ref, out_ref):
    rows = all_ref[...].astype(WIDE).reshape(SLOW * PER, CMP, PAIR)
    means = jnp.mean(rows, 1).astype(LOW)
    for y in range(FAST):
        out_ref[y, SUMS:, :] = means

    def one(z, carry):
        for y in range(FAST):
            at = (z * PER + jnp.minimum(table_ref[y * SLOW + z], PER - 1)) * BLK
            out_ref[y, pl.ds(pl.multiple_of(z * BLK, BLK), BLK), :] = all_ref[
                pl.ds(pl.multiple_of(at, BLK), BLK), :
            ]
        return carry

    lax.fori_loop(0, SLOW, one, 0)


def prep_kernel(q_ref, cot_ref, gates_ref, logs_ref, out_ref, msum_ref, msel_ref, ldsum_ref, ldsel_ref):
    cols = jnp.concatenate([gates_ref[0], gates_ref[1], logs_ref[0], logs_ref[1]], 0).T
    first = lax.broadcasted_iota(jnp.int32, (ROWS, PAIR), 1) < DH
    q = q_ref[...].astype(WIDE) * (DH ** (-0.5))
    heads_q = [jnp.where(first, q, 0.0).astype(LOW), jnp.where(first, pltpu.roll(q, DH, 1), 0.0).astype(LOW)]
    cot = cot_ref[...].astype(WIDE)
    for b in range(2):
        g = jnp.where(first, cols[:, 2 * b:2 * b + 1], cols[:, 2 * b + 1:2 * b + 2]) * cot
        terms = g * out_ref[b].astype(WIDE)
        heads_g = [jnp.where(first, 0.0, pltpu.roll(g, DH, 1)).astype(LOW), jnp.where(first, 0.0, g).astype(LOW)]
        deltas = [
            jnp.sum(jnp.where(first, terms, 0.0), -1, keepdims=True),
            jnp.sum(jnp.where(first, 0.0, terms), -1, keepdims=True),
        ]
        for h in range(2):
            ld = jnp.concatenate([cols[:, 4 + 2 * b + h:5 + 2 * b + h], deltas[h]], 1)
            if b == 0:
                msum_ref[h * ROWS:(h + 1) * ROWS, :] = heads_q[h]
                msum_ref[(2 + h) * ROWS:(3 + h) * ROWS, :] = heads_g[h]
                ldsum_ref[h * ROWS:(h + 1) * ROWS, :] = ld
            else:
                for s in range(SUB):
                    here = slice(s * SUB_ROWS, (s + 1) * SUB_ROWS)
                    msel_ref[s, h * SUB_ROWS:(h + 1) * SUB_ROWS, :] = heads_q[h][here]
                    msel_ref[s, (2 + h) * SUB_ROWS:(3 + h) * SUB_ROWS, :] = heads_g[h][here]
                    ldsel_ref[s, h * SUB_ROWS:(h + 1) * SUB_ROWS, :] = ld[here]


def main_kernel(place_ref, list_ref, msum_ref, msel_ref, ldsum_ref, ldsel_ref, arr_ref, hid_ref,
                dq_ref, ret_ref, kv_ref, hid_here, sem):
    load = pltpu.make_async_copy(hid_ref, hid_here, sem)
    load.start()
    base = place_ref[0] * ROWS
    scale = DH ** (-0.5)

    def grads(m, kv, seen, ld):
        half = m.shape[0] // 2
        sd = dot(m, kv, 1, 1)
        probs = jnp.where(seen, jnp.exp(sd[:half] - ld[:, :1]), 0.0)
        ds = (probs * (sd[half:] - ld[:, 1:2])).astype(LOW)
        weights = jnp.concatenate([ds, probs.astype(LOW)], 0)
        return dot(ds, kv, 1, 0), dot(weights, m, 0, 0)

    m = msum_ref[...]
    ld = ldsum_ref[...]
    row_at = lax.broadcasted_iota(jnp.int32, (2 * ROWS, 1), 0) & (ROWS - 1)
    per_fast = SLOW * PER
    step = 4
    lane = lax.broadcasted_iota(jnp.int32, (1, step * per_fast), 1)
    dq_sum = jnp.zeros((2 * ROWS, PAIR), WIDE)
    for y in range(0, FAST, step):
        kv = jnp.concatenate([arr_ref[y + k, SUMS:, :] for k in range(step)], 0)
        owner = (lane & (per_fast - 1)) // PER * FAST + y + lane // per_fast
        ends = (owner * PER + (lane & (PER - 1)) + 1) * CMP - 1 - base
        dq_part, kv_grad = grads(m, kv, ends <= row_at, ld)
        dq_sum += dq_part
        low = kv_grad.astype(LOW)
        for k in range(step):
            ret_ref[y + k, SUMS:PARTS, :] = low[k * per_fast:(k + 1) * per_fast]
    sub_at = lax.broadcasted_iota(jnp.int32, (2 * SUB_ROWS, 1), 0) & (SUB_ROWS - 1)
    sel_lane = lax.broadcasted_iota(jnp.int32, (1, TOPN * BLK), 1)
    for s in range(SUB):
        at_key = jnp.full((1, TOPN * BLK), FAR, jnp.int32)
        places = []
        for i in range(TOPN):
            n = list_ref[s * TOPN + i]
            live = n >= 0
            owner = jnp.maximum(n, 0) // PER
            fast = owner & (FAST - 1)
            at = pl.multiple_of(owner // FAST * BLK, BLK)
            places.append((live, fast, at))
            kv_ref[i * BLK:(i + 1) * BLK, :] = arr_ref[fast, pl.ds(at, BLK), :]
            start = jnp.where(live, n * BLK - base - i * BLK, FAR)
            at_key = jnp.where(sel_lane // BLK == i, start, at_key)
        kv = kv_ref[...]
        seen = at_key + sel_lane <= sub_at + s * SUB_ROWS
        dq_part, kv_grad = grads(msel_ref[s], kv, seen, ldsel_ref[s])
        low = kv_grad.astype(LOW)
        for i in range(TOPN):
            live, fast, at = places[i]

            @pl.when(live)
            def _(fast=fast, at=at, i=i):
                ret_ref[fast, pl.ds(at, BLK), :] = low[i * BLK:(i + 1) * BLK]

        top = s * SUB_ROWS
        for h in range(2):
            total = dq_sum[h * ROWS + top:h * ROWS + top + SUB_ROWS, :DH]
            total = total + dq_part[h * SUB_ROWS:(h + 1) * SUB_ROWS, :DH]
            dq_ref[top:top + SUB_ROWS, h * DH:(h + 1) * DH] = total * scale
    load.wait()
    qb = dq_ref[...].astype(LOW)
    span = FAST * COLS
    for z in range(SLOW):
        part = dot(hid_here[:, z * span:(z + 1) * span], qb, 0, 0).astype(LOW)
        for y in range(FAST):
            ret_ref[y, PARTS + z * COLS:PARTS + (z + 1) * COLS, :] = part[y * COLS:(y + 1) * COLS]


def merge_kernel(table_ref, in_ref, out_ref, tail_ref):
    tail = in_ref[0, SUMS:PARTS, :].astype(WIDE)
    for y in range(1, FAST):
        tail = tail + in_ref[y, SUMS:PARTS, :].astype(WIDE)
    tail_ref[:SLOW * PER, :] = tail
    tail_ref[SLOW * PER:, :] = jnp.zeros((8, PAIR), WIDE)

    def one(z, carry):
        sums = [jnp.zeros((BLK, PAIR), WIDE) for _ in range(PER)]
        cols = jnp.zeros((COLS, PAIR), WIDE)
        for y in range(FAST):
            pick = table_ref[y * SLOW + z]
            here = in_ref[y, pl.ds(pl.multiple_of(z * BLK, BLK), BLK), :].astype(WIDE)
            sums = [sums[b] + jnp.where(pick == b, here, 0.0) for b in range(PER)]
            cols = cols + in_ref[y, pl.ds(pl.multiple_of(PARTS + z * COLS, COLS), COLS), :].astype(WIDE)
        for b in range(PER):
            out_ref[z, b * BLK:(b + 1) * BLK, :] = sums[b].astype(LOW)
        out_ref[z, ROWS:ROWS + 8, :] = tail_ref[pl.ds(z * PER, 8), :].astype(LOW)
        out_ref[z, ROWS + 8:, :] = cols.astype(LOW)
        return carry

    lax.fori_loop(0, SLOW, one, 0)


def final_kernel(in_ref, gk_ref, gv_ref, gw_ref):
    total = in_ref[0].astype(WIDE)
    for z in range(1, SLOW):
        total = total + in_ref[z].astype(WIDE)
    rows = [
        total[b * BLK:(b + 1) * BLK] + total[ROWS + b:ROWS + b + 1] * (1.0 / CMP) for b in range(PER)
    ]
    turned = jnp.concatenate(rows, 0).T
    gk_ref[...] = turned[:DH]
    gv_ref[...] = turned[DH:]
    gw_ref[...] = total[ROWS + 8:]


def vmem():
    return pl.BlockSpec(memory_space=pltpu.VMEM)


def smem():
    return pl.BlockSpec(memory_space=pltpu.SMEM)


def shape(*sizes, kind=LOW):
    return jax.ShapeDtypeStruct(sizes, kind)


def call(kernel, ins, outs, scratch=()):
    many = isinstance(outs, tuple)
    return pl.pallas_call(
        kernel,
        out_shape=outs,
        in_specs=ins,
        out_specs=tuple(vmem() for _ in outs) if many else vmem(),
        scratch_shapes=list(scratch),
        name=kernel.__name__,
    )


def shards(queries, keys, values, hidden, log_sums, gates, branch_out, cotangent, chosen):
    slow_at = lax.axis_index(KV[0])
    fast_at = lax.axis_index(KV[1])
    place = slow_at * FAST + fast_at
    lists = chosen[:, 0]
    near = lax.dynamic_slice_in_dim(lists, slow_at * FAST, FAST, 0)
    owner = near // PER
    ours = (near >= 0) & (owner % FAST == fast_at)
    hits = ours[..., None] & ((owner // FAST)[..., None] == jnp.arange(SLOW, dtype=jnp.int32))
    table = jnp.min(jnp.where(hits, (near % PER)[..., None], PER), 1).reshape(-1)
    listing = lax.dynamic_index_in_dim(lists, place, 0, keepdims=False)

    pairs = call(pairs_kernel, [vmem(), vmem()], shape(ROWS, PAIR))(keys.T, values.T)
    along = lax.all_gather(pairs, KV[0], axis=0, tiled=True)
    outbound = call(relay_kernel, [smem(), vmem()], shape(FAST, FETCH, PAIR))(table, along)
    arrived = lax.all_to_all(outbound, KV[1], split_axis=0, concat_axis=0, tiled=True)

    m_sum, m_sel, ld_sum, ld_sel = call(
        prep_kernel,
        [vmem()] * 5,
        (
            shape(4 * ROWS, PAIR),
            shape(SUB, 4 * SUB_ROWS, PAIR),
            shape(2 * ROWS, 2, kind=WIDE),
            shape(SUB, 2 * SUB_ROWS, 2, kind=WIDE),
        ),
    )(queries, cotangent, jnp.transpose(gates, (0, 2, 1)), jnp.transpose(log_sums, (0, 2, 1)), branch_out)
    grad_queries, returned = call(
        main_kernel,
        [smem(), smem()] + [vmem()] * 5 + [pl.BlockSpec(memory_space=pl.ANY)],
        (shape(ROWS, PAIR, kind=WIDE), shape(FAST, BACK, PAIR)),
        (
            pltpu.VMEM((TOPN * BLK, PAIR), LOW),
            pltpu.VMEM(hidden.shape, LOW),
            pltpu.SemaphoreType.DMA,
        ),
    )(place[None], listing, m_sum, m_sel, ld_sum, ld_sel, arrived, hidden)
    across = lax.all_to_all(returned, KV[1], split_axis=0, concat_axis=0, tiled=True)
    merged = call(
        merge_kernel,
        [smem(), vmem()],
        shape(SLOW, LAST, PAIR),
        (pltpu.VMEM((SLOW * PER + 8, PAIR), WIDE),),
    )(table, across)
    home = lax.all_to_all(merged, KV[0], split_axis=0, concat_axis=0, tiled=True)
    turned_keys, turned_values, grad_weight = call(
        final_kernel,
        [vmem()],
        (shape(DH, ROWS, kind=WIDE), shape(DH, ROWS, kind=WIDE), shape(COLS, PAIR, kind=WIDE)),
    )(home)
    return (grad_queries, turned_keys.T, turned_values.T, grad_weight)


def solution(mesh):
    finer = Mesh(mesh.devices.reshape(SLOW, FAST, mesh.shape["tp"]), ("kv_0", "kv_1", "tp"))
    placed = (
        P(KV, "tp"),
        P(KV, "tp"),
        P(KV, "tp"),
        P(KV, None),
        P(None, KV, "tp"),
        P(None, KV, "tp"),
        P(None, KV, "tp"),
        P(KV, "tp"),
        P(None, "tp", None),
    )
    return jax.shard_map(
        shards,
        mesh=finer,
        in_specs=placed,
        out_specs=(P(KV, "tp"), P(KV, "tp"), P(KV, "tp"), P(KV, "tp")),
        check_vma=False,
    )
```

time: 227 us -> 175 us (0.77)
  waiting for transfers between devices: 119 us -> 21.3 us
  blocking collectives: 41 us -> 124 us
  starting transfers between devices: 32.7 us -> 7.1 us
  local copies, waits for them, and re-layouts: 12.3 us -> 3.19 us
  other arithmetic: 5.27 us -> 0.26 us
  Pallas kernels: 13.6 us -> 17.4 us
    all_to_all x2 -> x1, waiting for transfers between devices: 119 us -> 21.3 us  [shards(): lax.all_to_all(outbound, KV[1], split_axis=0, concat_axis=0, tiled=True)]
    all_gather x0 -> x1, blocking collectives: none -> 47.8 us  [shards(): along = lax.all_gather(pairs, KV[0], axis=0, tiled=True)]
    all_to_all x2, blocking collectives: 41 us -> 76.4 us  [the longest x1 41 us: shards(): lax.all_to_all(returned, KV[1], split_axis=0, concat_axis=0, tiled=True)]
    all_to_all x2 -> x1, starting transfers between devices: 32.7 us -> 7.1 us  [shards(): lax.all_to_all(outbound, KV[1], split_axis=0, concat_axis=0, tiled=True)]
    unnamed x27 -> x5, local copies, waits for them, and re-layouts: 8.72 us -> 1.83 us
    pallas_call x4 -> x6, Pallas kernels: 13.6 us -> 17.4 us  [the longest x1 6.1 us: shards(): call(main_kernel, [smem(), smem()] + [vmem()] * 5 + [pl.BlockSpec(memory_...]
  transfers between devices with their start and end apart: 2 -> 1, of which waited for: 2 -> 1; matrix products, arithmetic and copies ran while one was open for 3% -> 0% of each run, Pallas kernels for 0% -> 1%
where the time goes in v2:
time: 175 us; the launch traced here: 174 us
  blocking collectives  124 us (71%)
  waiting for transfers between devices  21.3 us (12%)
  Pallas kernels  17.4 us (10%)
  starting transfers between devices  7.1 us (4%)
  local copies, waits for them, and re-layouts  3.19 us (2%)
    all_gather x1, blocking collectives, shards(): along = lax.all_gather(pairs, KV[0], axis=0, tiled=True)  47.8 us
    all_to_all x1, blocking collectives, shards(): lax.all_to_all(returned, KV[1], split_axis=0, concat_axis=0, tiled=True)  41 us
    all_to_all x1, blocking collectives, shards(): lax.all_to_all(merged, KV[0], split_axis=0, concat_axis=0, tiled=True)  35.5 us
    all_to_all x1, waiting for transfers between devices, shards(): lax.all_to_all(outbound, KV[1], split_axis=0, concat_axis=0, tiled=True)  21.3 us
    all_to_all x1, starting transfers between devices, shards(): lax.all_to_all(outbound, KV[1], split_axis=0, concat_axis=0, tiled=True)  7.1 us
    pallas_call x1, Pallas kernels, shards(): call(main_kernel, [smem(), smem()] + [vmem()] * 5 + [pl.BlockSpec(memory_...  6.1 us
  transfers between devices with their start and end apart: 1, of which 1 were waited for; matrix products, arithmetic and copies ran while one was open for 0% of the time, Pallas kernels for 1%

profile of v2, /device:TPU:6, one launch (start us, length us, event | category | flops | bytes accessed | tf_op | source)
XLA Modules:
  0.0 174.2 jit_solution(3299202264452828535)
XLA Ops:
  0.6 0.0 copy-start
  0.7 0.7 copy-done
  1.4 0.1 constant_dynamic-slice_fusion
  1.4 0.1 copy.31
  1.6 0.2 select_reduce_fusion
  1.8 0.6 reshape.104.table_ref
  2.4 1.5 pairs_kernel.1
  3.8 47.8 %all_gather.3.all_ref = bf16[2048,128]{1,0:T(8,128)(2,1)} all-gather(bf16[128,128]{1,0:T(8,128)(2,1)} %pairs_kernel.1), channel_id=1, replica_groups=mesh['kv_0'=16,'kv_1'=8,'tp'=8] {'kv_0'}, dimensions={0}, use_global_device_ids=true | all-gather | bytes 557056 | tf_op jit(solution)/shard_map/all_gather | solution.py:231
  51.7 2.6 %relay_kernel.1 = bf16[8,576,128]{2,1,0:T(8,128)(2,1)} custom-call(s32[128]{0:T(128)} %reshape.104.table_ref, bf16[2048,128]{1,0:T(8,128)(2,1)} %all_gather.3.all_ref), custom_call_target="tpu_custom_call" | custom-call | tf_op jit(solution)/shard_map/relay_kernel/pallas_call | solution.py:232
  54.3 7.1 %all-to-all-start = ((bf16[8,576,128]{2,1,0:T(8,128)(2,1)}), bf16[8,576,128]{2,1,0:T(8,128)(2,1)S(1)}, u32[]{:S(2)}, u32[]{:S(2)}) async-start(bf16[8,576,128]{2,1,0:T(8,128)(2,1)} %relay_kernel.1), calls=%async_computation | async-start | bytes 2359296 | tf_op jit(solution)/shard_map/all_to_all | solution.py:233
  61.4 2.2 %prep_kernel.1 = (bf16[512,128]{1,0:T(8,128)(2,1)}, bf16[4,128,128]{2,1,0:T(8,128)(2,1)}, f32[256,2]{1,0:T(8,128)}, f32[4,64,2]{2,1,0:T(8,128)}) custom-call(bf16[128,128]{1,0:T(8,128)(2,1)} %q_ref.1, bf16[128,128]{1,0:T(8,128)(2,1)} %cot_ref.1, f32[2,2,128]{2,1,0:T(2,128)} %bitcast.42, f32[2,2,128]{2,1,0:T(2,128)} %bitcast.43, bf16[2,128,128]{2,1,0:T(8,128)(2,1)} %out_ref.1), custom_call_target="tpu_custom_call" | custom-call | tf_op jit(solution)/shard_map/prep_kernel/pallas_call | solution.py:235
  63.6 0.7 dynamic-slice_reduce_fusion.list_ref
  64.3 21.3 %all-to-all-done.arr_ref = bf16[8,576,128]{2,1,0:T(8,128)(2,1)S(1)} async-done(((bf16[8,576,128]{2,1,0:T(8,128)(2,1)}), bf16[8,576,128]{2,1,0:T(8,128)(2,1)S(1)}, u32[]{:S(2)}, u32[]{:S(2)}) %all-to-all-start) | async-done | bytes 1179680 | tf_op jit(solution)/shard_map/all_to_all | solution.py:233
  85.6 0.0 copy-start.1
  85.6 1.0 copy-done.1
  86.6 6.1 %main_kernel.1 = (f32[128,128]{1,0:T(8,128)}, bf16[8,832,128]{2,1,0:T(8,128)(2,1)}) custom-call(s32[1]{0:T(128)} %bitcast.place_ref, s32[48]{0:T(128)} %dynamic-slice_reduce_fusion.list_ref, bf16[512,128]{1,0:T(8,128)(2,1)} %get-tuple-element.13.msum_ref, bf16[4,128,128]{2,1,0:T(8,128)(2,1)} %get-tuple-element.14.msel_ref, ...), custom_call_target="tpu_custom_call" | custom-call | tf_op jit(solution)/shard_map/main_kernel/pallas_call | solution.py:245
  92.8 41.0 %all_to_all.15.in_ref = bf16[8,832,128]{2,1,0:T(8,128)(2,1)} all-to-all(bf16[8,832,128]{2,1,0:T(8,128)(2,1)} %get-tuple-element.18), channel_id=1, replica_groups=mesh['kv_0'=16,'kv_1'=8,'tp'=8] {'kv_1'}, dimensions={0} | all-to-all | bytes 3407872 | tf_op jit(solution)/shard_map/all_to_all | solution.py:255
  133.7 3.2 %merge_kernel.1 = bf16[16,152,128]{2,1,0:T(8,128)(2,1)} custom-call(s32[128]{0:T(128)} %reshape.104.table_ref, bf16[8,832,128]{2,1,0:T(8,128)(2,1)} %all_to_all.15.in_ref), custom_call_target="tpu_custom_call" | custom-call | tf_op jit(solution)/shard_map/merge_kernel/pallas_call | solution.py:256
  136.9 35.5 %all_to_all.16.in_ref = bf16[16,152,128]{2,1,0:T(8,128)(2,1)} all-to-all(bf16[16,152,128]{2,1,0:T(8,128)(2,1)} %merge_kernel.1), channel_id=1, replica_groups=mesh['kv_0'=16,'kv_1'=8,'tp'=8] {'kv_0'}, dimensions={0} | all-to-all | bytes 1245184 | tf_op jit(solution)/shard_map/all_to_all | solution.py:262
  172.4 1.8 %final_kernel.1 = (f32[64,128]{1,0:T(8,128)}, f32[64,128]{1,0:T(8,128)}, f32[16,128]{1,0:T(8,128)}) custom-call(bf16[16,152,128]{2,1,0:T(8,128)(2,1)} %all_to_all.16.in_ref), custom_call_target="tpu_custom_call" | custom-call | tf_op jit(solution)/shard_map/final_kernel/pallas_call | solution.py:263
  (2 shorter events, 0.0 us)
Async XLA Ops:
  0.6 0.7 copy-start
  54.3 31.3 %all-to-all-start = ((bf16[8,576,128]{2,1,0:T(8,128)(2,1)}), bf16[8,576,128]{2,1,0:T(8,128)(2,1)S(1)}, u32[]{:S(2)}, u32[]{:S(2)}) async-start(bf16[8,576,128]{2,1,0:T(8,128)(2,1)} %relay_kernel.1), calls=%async_computation | async-start | bytes 2359296 | tf_op jit(solution)/shard_map/all_to_all | solution.py:233
  85.6 1.0 copy-start.1

commit v3 on v2

--- a/solution.py
+++ b/solution.py
@@ -33,26 +33,38 @@
     return lax.dot_general(a, b, (((ca,), (cb,)), ((), ())), preferred_element_type=WIDE)
 
 
-def pairs_kernel(keys_ref, values_ref, out_ref):
+def pairs_kernel(place_ref, keys_ref, values_ref, chosen_ref, out_ref, table_ref):
     both = jnp.concatenate([keys_ref[...], values_ref[...]], 0).astype(WIDE)
     out_ref[...] = both.T.astype(LOW)
-
-
-def relay_kernel(table_ref, all_ref, out_ref):
-    rows = all_ref[...].astype(WIDE).reshape(SLOW * PER, CMP, PAIR)
-    means = jnp.mean(rows, 1).astype(LOW)
-    for y in range(FAST):
-        out_ref[y, SUMS:, :] = means
-
-    def one(z, carry):
-        for y in range(FAST):
-            at = (z * PER + jnp.minimum(table_ref[y * SLOW + z], PER - 1)) * BLK
-            out_ref[y, pl.ds(pl.multiple_of(z * BLK, BLK), BLK), :] = all_ref[
-                pl.ds(pl.multiple_of(at, BLK), BLK), :
-            ]
-        return carry
-
-    lax.fori_loop(0, SLOW, one, 0)
+    entry = chosen_ref[...]
+    fast_at = place_ref[0] & (FAST - 1)
+    owner = jnp.where(entry >= 0, entry // PER, -1)
+    inner = entry & (PER - 1)
+    for z in range(SLOW):
+        hit = jnp.where(owner == z * FAST + fast_at, inner, PER)
+        table_ref[z:z + 1, :] = jnp.min(hit, 0, keepdims=True)
+
+
+def relay_kernel(place_ref, table_ref, all_ref, out_ref, mean_ref):
+    step = pl.program_id(0)
+    per_step = out_ref.shape[0]
+    column = place_ref[0] // FAST * FAST
+
+    @pl.when(step == 0)
+    def _():
+        rows = all_ref[...].astype(WIDE).reshape(SLOW * PER, CMP, PAIR)
+        mean_ref[...] = jnp.mean(rows, 1).astype(LOW)
+
+    for k in range(per_step):
+        out_ref[k, SUMS:, :] = mean_ref[...]
+
+        def one(z, carry, k=k):
+            pick = jnp.minimum(table_ref[z, column + step * per_step + k], PER - 1)
+            at = pl.multiple_of((z * PER + pick) * BLK, BLK)
+            out_ref[k, pl.ds(pl.multiple_of(z * BLK, BLK), BLK), :] = all_ref[pl.ds(at, BLK), :]
+            return carry
+
+        lax.fori_loop(0, SLOW, one, 0, unroll=4)
 
 
 def prep_kernel(q_ref, cot_ref, gates_ref, logs_ref, out_ref, msum_ref, msel_ref, ldsum_ref, ldsel_ref):
@@ -84,9 +96,13 @@
 
 
 def main_kernel(place_ref, list_ref, msum_ref, msel_ref, ldsum_ref, ldsel_ref, arr_ref, hid_ref,
-                dq_ref, ret_ref, kv_ref, hid_here, sem):
-    load = pltpu.make_async_copy(hid_ref, hid_here, sem)
-    load.start()
+                dq_ref, out_ref, kv_ref, hid_here, arr_here, ret_ref, sems):
+    load_sums = pltpu.make_async_copy(arr_ref.at[:, SUMS:], arr_here.at[:, SUMS:], sems.at[0])
+    load_sums.start()
+    load_blocks = pltpu.make_async_copy(arr_ref.at[:, :SUMS], arr_here.at[:, :SUMS], sems.at[1])
+    load_blocks.start()
+    load_hidden = pltpu.make_async_copy(hid_ref, hid_here, sems.at[2])
+    load_hidden.start()
     base = place_ref[0] * ROWS
     scale = DH ** (-0.5)
 
@@ -105,8 +121,9 @@
     step = 4
     lane = lax.broadcasted_iota(jnp.int32, (1, step * per_fast), 1)
     dq_sum = jnp.zeros((2 * ROWS, PAIR), WIDE)
+    load_sums.wait()
     for y in range(0, FAST, step):
-        kv = jnp.concatenate([arr_ref[y + k, SUMS:, :] for k in range(step)], 0)
+        kv = jnp.concatenate([arr_here[y + k, SUMS:, :] for k in range(step)], 0)
         owner = (lane & (per_fast - 1)) // PER * FAST + y + lane // per_fast
         ends = (owner * PER + (lane & (PER - 1)) + 1) * CMP - 1 - base
         dq_part, kv_grad = grads(m, kv, ends <= row_at, ld)
@@ -114,6 +131,7 @@
         low = kv_grad.astype(LOW)
         for k in range(step):
             ret_ref[y + k, SUMS:PARTS, :] = low[k * per_fast:(k + 1) * per_fast]
+    load_blocks.wait()
     sub_at = lax.broadcasted_iota(jnp.int32, (2 * SUB_ROWS, 1), 0) & (SUB_ROWS - 1)
     sel_lane = lax.broadcasted_iota(jnp.int32, (1, TOPN * BLK), 1)
     for s in range(SUB):
@@ -126,7 +144,7 @@
             fast = owner & (FAST - 1)
             at = pl.multiple_of(owner // FAST * BLK, BLK)
             places.append((live, fast, at))
-            kv_ref[i * BLK:(i + 1) * BLK, :] = arr_ref[fast, pl.ds(at, BLK), :]
+            kv_ref[i * BLK:(i + 1) * BLK, :] = arr_here[fast, pl.ds(at, BLK), :]
             start = jnp.where(live, n * BLK - base - i * BLK, FAR)
             at_key = jnp.where(sel_lane // BLK == i, start, at_key)
         kv = kv_ref[...]
@@ -145,50 +163,76 @@
             total = dq_sum[h * ROWS + top:h * ROWS + top + SUB_ROWS, :DH]
             total = total + dq_part[h * SUB_ROWS:(h + 1) * SUB_ROWS, :DH]
             dq_ref[top:top + SUB_ROWS, h * DH:(h + 1) * DH] = total * scale
-    load.wait()
+    store_first = pltpu.make_async_copy(ret_ref.at[:, :PARTS], out_ref.at[:, :PARTS], sems.at[3])
+    store_first.start()
+    load_hidden.wait()
     qb = dq_ref[...].astype(LOW)
     span = FAST * COLS
     for z in range(SLOW):
         part = dot(hid_here[:, z * span:(z + 1) * span], qb, 0, 0).astype(LOW)
         for y in range(FAST):
             ret_ref[y, PARTS + z * COLS:PARTS + (z + 1) * COLS, :] = part[y * COLS:(y + 1) * COLS]
-
-
-def merge_kernel(table_ref, in_ref, out_ref, tail_ref):
-    tail = in_ref[0, SUMS:PARTS, :].astype(WIDE)
-    for y in range(1, FAST):
-        tail = tail + in_ref[y, SUMS:PARTS, :].astype(WIDE)
-    tail_ref[:SLOW * PER, :] = tail
-    tail_ref[SLOW * PER:, :] = jnp.zeros((8, PAIR), WIDE)
-
-    def one(z, carry):
+    store_rest = pltpu.make_async_copy(ret_ref.at[:, PARTS:], out_ref.at[:, PARTS:], sems.at[4])
+    store_rest.start()
+    store_first.wait()
+    store_rest.wait()
+
+
+def merge_kernel(place_ref, table_ref, in_ref, sums_ref, parts_ref, out_ref, tail_ref):
+    step = pl.program_id(0)
+    per_step = out_ref.shape[0]
+    column = place_ref[0] // FAST * FAST
+
+    @pl.when(step == 0)
+    def _():
+        tail = sums_ref[0].astype(WIDE)
+        for y in range(1, FAST):
+            tail = tail + sums_ref[y].astype(WIDE)
+        tail_ref[:SLOW * PER, :] = tail
+        tail_ref[SLOW * PER:, :] = jnp.zeros((8, PAIR), WIDE)
+
+    def one(k, carry):
+        z = step * per_step + k
         sums = [jnp.zeros((BLK, PAIR), WIDE) for _ in range(PER)]
         cols = jnp.zeros((COLS, PAIR), WIDE)
         for y in range(FAST):
-            pick = table_ref[y * SLOW + z]
-            here = in_ref[y, pl.ds(pl.multiple_of(z * BLK, BLK), BLK), :].astype(WIDE)
+            pick = table_ref[z, column + y]
+            here = in_ref[y, pl.ds(pl.multiple_of(k * BLK, BLK), BLK), :].astype(WIDE)
             sums = [sums[b] + jnp.where(pick == b, here, 0.0) for b in range(PER)]
-            cols = cols + in_ref[y, pl.ds(pl.multiple_of(PARTS + z * COLS, COLS), COLS), :].astype(WIDE)
+            cols = cols + parts_ref[y, pl.ds(pl.multiple_of(k * COLS, COLS), COLS), :].astype(WIDE)
         for b in range(PER):
-            out_ref[z, b * BLK:(b + 1) * BLK, :] = sums[b].astype(LOW)
-        out_ref[z, ROWS:ROWS + 8, :] = tail_ref[pl.ds(z * PER, 8), :].astype(LOW)
-        out_ref[z, ROWS + 8:, :] = cols.astype(LOW)
+            out_ref[k, b * BLK:(b + 1) * BLK, :] = sums[b].astype(LOW)
+        out_ref[k, ROWS:ROWS + 8, :] = tail_ref[pl.ds(z * PER, 8), :].astype(LOW)
+        out_ref[k, ROWS + 8:, :] = cols.astype(LOW)
         return carry
 
-    lax.fori_loop(0, SLOW, one, 0)
-
-
-def final_kernel(in_ref, gk_ref, gv_ref, gw_ref):
-    total = in_ref[0].astype(WIDE)
-    for z in range(1, SLOW):
-        total = total + in_ref[z].astype(WIDE)
-    rows = [
-        total[b * BLK:(b + 1) * BLK] + total[ROWS + b:ROWS + b + 1] * (1.0 / CMP) for b in range(PER)
-    ]
-    turned = jnp.concatenate(rows, 0).T
-    gk_ref[...] = turned[:DH]
-    gv_ref[...] = turned[DH:]
-    gw_ref[...] = total[ROWS + 8:]
+    lax.fori_loop(0, per_step, one, 0)
+
+
+def final_kernel(in_ref, gk_ref, gv_ref, gw_ref, total_ref):
+    step = pl.program_id(0)
+    part = in_ref[0].astype(WIDE)
+    for z in range(1, in_ref.shape[0]):
+        part = part + in_ref[z].astype(WIDE)
+
+    @pl.when(step == 0)
+    def _():
+        total_ref[...] = part
+
+    @pl.when(step > 0)
+    def _():
+        total_ref[...] += part
+
+    @pl.when(step == pl.num_programs(0) - 1)
+    def _():
+        total = total_ref[...]
+        rows = [
+            total[b * BLK:(b + 1) * BLK] + total[ROWS + b:ROWS + b + 1] * (1.0 / CMP) for b in range(PER)
+        ]
+        turned = jnp.concatenate(rows, 0).T
+        gk_ref[...] = turned[:DH]
+        gv_ref[...] = turned[DH:]
+        gw_ref[...] = total[ROWS + 8:]
 
 
 def vmem():
@@ -203,35 +247,44 @@
     return jax.ShapeDtypeStruct(sizes, kind)
 
 
-def call(kernel, ins, outs, scratch=()):
-    many = isinstance(outs, tuple)
+def piece(sizes, at):
+    return pl.BlockSpec(sizes, at)
+
+
+def call(kernel, ins, outs, specs, scratch=(), grid=()):
     return pl.pallas_call(
         kernel,
+        grid=grid,
         out_shape=outs,
         in_specs=ins,
-        out_specs=tuple(vmem() for _ in outs) if many else vmem(),
+        out_specs=specs,
         scratch_shapes=list(scratch),
         name=kernel.__name__,
     )
 
 
 def shards(queries, keys, values, hidden, log_sums, gates, branch_out, cotangent, chosen):
-    slow_at = lax.axis_index(KV[0])
-    fast_at = lax.axis_index(KV[1])
-    place = slow_at * FAST + fast_at
+    place = lax.axis_index(KV)
+    here = place[None]
     lists = chosen[:, 0]
-    near = lax.dynamic_slice_in_dim(lists, slow_at * FAST, FAST, 0)
-    owner = near // PER
-    ours = (near >= 0) & (owner % FAST == fast_at)
-    hits = ours[..., None] & ((owner // FAST)[..., None] == jnp.arange(SLOW, dtype=jnp.int32))
-    table = jnp.min(jnp.where(hits, (near % PER)[..., None], PER), 1).reshape(-1)
+    pairs, table = call(
+        pairs_kernel,
+        [smem(), vmem(), vmem(), vmem()],
+        (shape(ROWS, PAIR), shape(SLOW, lists.shape[0], kind=jnp.int32)),
+        (vmem(), vmem()),
+    )(here, keys.T, values.T, lists.T)
+    along = lax.all_gather(pairs, KV[0], axis=0, tiled=True)
+    outbound = call(
+        relay_kernel,
+        [smem(), smem(), piece((SLOW * ROWS, PAIR), lambda i: (0, 0))],
+        shape(FAST, FETCH, PAIR),
+        piece((FAST // 4, FETCH, PAIR), lambda i: (i, 0, 0)),
+        (pltpu.VMEM((SLOW * PER, PAIR), LOW),),
+        grid=(4,),
+    )(here, table, along)
+    arrived = lax.all_to_all(outbound, KV[1], split_axis=0, concat_axis=0, tiled=True)
+
     listing = lax.dynamic_index_in_dim(lists, place, 0, keepdims=False)
-
-    pairs = call(pairs_kernel, [vmem(), vmem()], shape(ROWS, PAIR))(keys.T, values.T)
-    along = lax.all_gather(pairs, KV[0], axis=0, tiled=True)
-    outbound = call(relay_kernel, [smem(), vmem()], shape(FAST, FETCH, PAIR))(table, along)
-    arrived = lax.all_to_all(outbound, KV[1], split_axis=0, concat_axis=0, tiled=True)
-
     m_sum, m_sel, ld_sum, ld_sel = call(
         prep_kernel,
         [vmem()] * 5,
@@ -241,29 +294,46 @@
             shape(2 * ROWS, 2, kind=WIDE),
             shape(SUB, 2 * SUB_ROWS, 2, kind=WIDE),
         ),
+        (vmem(),) * 4,
     )(queries, cotangent, jnp.transpose(gates, (0, 2, 1)), jnp.transpose(log_sums, (0, 2, 1)), branch_out)
     grad_queries, returned = call(
         main_kernel,
-        [smem(), smem()] + [vmem()] * 5 + [pl.BlockSpec(memory_space=pl.ANY)],
+        [smem(), smem()] + [vmem()] * 4 + [pl.BlockSpec(memory_space=pl.ANY)] * 2,
         (shape(ROWS, PAIR, kind=WIDE), shape(FAST, BACK, PAIR)),
+        (vmem(), pl.BlockSpec(memory_space=pl.ANY)),
         (
             pltpu.VMEM((TOPN * BLK, PAIR), LOW),
             pltpu.VMEM(hidden.shape, LOW),
-            pltpu.SemaphoreType.DMA,
+            pltpu.VMEM((FAST, FETCH, PAIR), LOW),
+            pltpu.VMEM((FAST, BACK, PAIR), LOW),
+            pltpu.SemaphoreType.DMA((5,)),
         ),
-    )(place[None], listing, m_sum, m_sel, ld_sum, ld_sel, arrived, hidden)
+    )(here, listing, m_sum, m_sel, ld_sum, ld_sel, arrived, hidden)
     across = lax.all_to_all(returned, KV[1], split_axis=0, concat_axis=0, tiled=True)
+    per_step = SLOW // 4
     merged = call(
         merge_kernel,
-        [smem(), vmem()],
+        [
+            smem(),
+            smem(),
+            piece((FAST, per_step * BLK, PAIR), lambda i: (0, i, 0)),
+            piece((FAST, SLOW * PER, PAIR), lambda i: (0, SUMS // (SLOW * PER), 0)),
+            piece((FAST, per_step * COLS, PAIR), lambda i: (0, PARTS // (per_step * COLS) + i, 0)),
+        ],
         shape(SLOW, LAST, PAIR),
+        piece((per_step, LAST, PAIR), lambda i: (i, 0, 0)),
         (pltpu.VMEM((SLOW * PER + 8, PAIR), WIDE),),
-    )(table, across)
+        grid=(4,),
+    )(here, table, across, across, across)
     home = lax.all_to_all(merged, KV[0], split_axis=0, concat_axis=0, tiled=True)
+    whole = lambda i: (0, 0)
     turned_keys, turned_values, grad_weight = call(
         final_kernel,
-        [vmem()],
+        [piece((SLOW // 4, LAST, PAIR), lambda i: (i, 0, 0))],
         (shape(DH, ROWS, kind=WIDE), shape(DH, ROWS, kind=WIDE), shape(COLS, PAIR, kind=WIDE)),
+        (piece((DH, ROWS), whole), piece((DH, ROWS), whole), piece((COLS, PAIR), whole)),
+        (pltpu.VMEM((LAST, PAIR), WIDE),),
+        grid=(4,),
     )(home)
     return (grad_queries, turned_keys.T, turned_values.T, grad_weight)
 

time: 175 us -> 176 us (level)
  Pallas kernels: 17.4 us -> 20.8 us
    pallas_call x5, Pallas kernels: 15.2 us -> 18.6 us  [the longest x1 7.14 us: shards(): call(main_kernel, [smem(), smem()] + [vmem()] * 4 + [pl.BlockSpec(memory_...]
where the time goes in v3:
time: 176 us
  blocking collectives  124 us (70%)
  waiting for transfers between devices  21.3 us (12%)
  Pallas kernels  20.8 us (12%)
  starting transfers between devices  7.1 us (4%)
    all_gather x1, blocking collectives, shards(): along = lax.all_gather(pairs, KV[0], axis=0, tiled=True)  47.8 us
    all_to_all x1, blocking collectives, shards(): lax.all_to_all(returned, KV[1], split_axis=0, concat_axis=0, tiled=True)  41 us
    all_to_all x1, blocking collectives, shards(): lax.all_to_all(merged, KV[0], split_axis=0, concat_axis=0, tiled=True)  35.5 us
    all_to_all x1, waiting for transfers between devices, shards(): lax.all_to_all(outbound, KV[1], split_axis=0, concat_axis=0, tiled=True)  21.3 us
    pallas_call x1, Pallas kernels, shards(): call(main_kernel, [smem(), smem()] + [vmem()] * 4 + [pl.BlockSpec(memory_...  7.14 us
    all_to_all x1, starting transfers between devices, shards(): lax.all_to_all(outbound, KV[1], split_axis=0, concat_axis=0, tiled=True)  7.1 us
    pallas_call x1, Pallas kernels, shards(): call(merge_kernel, [smem(), smem(), piece((FAST, per_step * BLK, PAIR), l...  3.96 us
  transfers between devices with their start and end apart: 1, of which 1 were waited for; matrix products, arithmetic and copies ran while one was open for 0% of the time, Pallas kernels for 1%

profile of v3, /device:TPU:6, one launch (start us, length us, event | category | flops | bytes accessed | tf_op | source)
XLA Modules:
  0.0 175.9 jit_solution(13634886401978968981)
XLA Ops:
  0.6 1.5 pairs_kernel.1
  2.1 47.8 %all_gather.3.all_ref = bf16[2048,128]{1,0:T(8,128)(2,1)} all-gather(bf16[128,128]{1,0:T(8,128)(2,1)} %get-tuple-element.20), channel_id=1, replica_groups=mesh['kv_0'=16,'kv_1'=8,'tp'=8] {'kv_0'}, dimensions={0}, use_global_device_ids=true | all-gather | bytes 557056 | tf_op jit(solution)/shard_map/all_gather | solution.py:276
  50.0 0.0 copy-start.1
  50.0 3.3 %relay_kernel.1 = bf16[8,576,128]{2,1,0:T(8,128)(2,1)} custom-call(s32[1]{0:T(128)} %bitcast.place_ref, s32[16,128]{1,0:T(8,128)} %get-tuple-element.19.table_ref, bf16[2048,128]{1,0:T(8,128)(2,1)} %all_gather.3.all_ref), custom_call_target="tpu_custom_call" | custom-call | tf_op jit(solution)/shard_map/relay_kernel/pallas_call | solution.py:277
  53.3 7.1 %all-to-all-start = ((bf16[8,576,128]{2,1,0:T(8,128)(2,1)}), bf16[8,576,128]{2,1,0:T(8,128)(2,1)S(1)}, u32[]{:S(2)}, u32[]{:S(2)}) async-start(bf16[8,576,128]{2,1,0:T(8,128)(2,1)} %relay_kernel.1), calls=%async_computation | async-start | bytes 2359296 | tf_op jit(solution)/shard_map/all_to_all | solution.py:285
  60.4 2.2 %prep_kernel.1 = (bf16[512,128]{1,0:T(8,128)(2,1)}, bf16[4,128,128]{2,1,0:T(8,128)(2,1)}, f32[256,2]{1,0:T(8,128)}, f32[4,64,2]{2,1,0:T(8,128)}) custom-call(bf16[128,128]{1,0:T(8,128)(2,1)} %q_ref.1, bf16[128,128]{1,0:T(8,128)(2,1)} %cot_ref.1, f32[2,2,128]{2,1,0:T(2,128)} %bitcast.13, f32[2,2,128]{2,1,0:T(2,128)} %bitcast.14, bf16[2,128,128]{2,1,0:T(8,128)(2,1)} %out_ref.1), custom_call_target="tpu_custom_call" | custom-call | tf_op jit(solution)/shard_map/prep_kernel/pallas_call | solution.py:288
  62.6 0.0 copy-done.1
  62.6 0.7 dynamic-slice_reduce_fusion.list_ref
  63.3 21.3 %all-to-all-done.arr_ref = bf16[8,576,128]{2,1,0:T(8,128)(2,1)S(1)} async-done(((bf16[8,576,128]{2,1,0:T(8,128)(2,1)}), bf16[8,576,128]{2,1,0:T(8,128)(2,1)S(1)}, u32[]{:S(2)}, u32[]{:S(2)}) %all-to-all-start) | async-done | bytes 1179680 | tf_op jit(solution)/shard_map/all_to_all | solution.py:285
  84.6 0.0 copy-start
  84.6 1.0 copy-done
  85.6 7.1 %main_kernel.1 = (f32[128,128]{1,0:T(8,128)}, bf16[8,832,128]{2,1,0:T(8,128)(2,1)}) custom-call(s32[1]{0:T(128)} %bitcast.place_ref, s32[48]{0:T(128)} %dynamic-slice_reduce_fusion.list_ref, bf16[512,128]{1,0:T(8,128)(2,1)} %get-tuple-element.15.msum_ref, bf16[4,128,128]{2,1,0:T(8,128)(2,1)} %get-tuple-element.16.msel_ref, ...), custom_call_target="tpu_custom_call" | custom-call | tf_op jit(solution)/shard_map/main_kernel/pallas_call | solution.py:299
  92.8 41.0 %all_to_all.15.in_ref.sums_ref.parts_ref = bf16[8,832,128]{2,1,0:T(8,128)(2,1)} all-to-all(bf16[8,832,128]{2,1,0:T(8,128)(2,1)} %get-tuple-element.22), channel_id=1, replica_groups=mesh['kv_0'=16,'kv_1'=8,'tp'=8] {'kv_1'}, dimensions={0} | all-to-all | bytes 3407872 | tf_op jit(solution)/shard_map/all_to_all | solution.py:312
  133.7 4.0 %merge_kernel.1 = bf16[16,152,128]{2,1,0:T(8,128)(2,1)} custom-call(s32[1]{0:T(128)} %bitcast.place_ref, s32[16,128]{1,0:T(8,128)} %get-tuple-element.19.table_ref, bf16[8,832,128]{2,1,0:T(8,128)(2,1)} %all_to_all.15.in_ref.sums_ref.parts_ref, bf16[8,832,128]{2,1,0:T(8,128)(2,1)} %all_to_all.15.in_ref.sums_ref.parts_ref, ...), custom_call_target="tpu_custom_call" | custom-call | tf_op jit(solution)/shard_map/merge_kernel/pallas_call | solution.py:314
  137.7 35.5 %all_to_all.16.in_ref = bf16[16,152,128]{2,1,0:T(8,128)(2,1)} all-to-all(bf16[16,152,128]{2,1,0:T(8,128)(2,1)} %merge_kernel.1), channel_id=1, replica_groups=mesh['kv_0'=16,'kv_1'=8,'tp'=8] {'kv_0'}, dimensions={0} | all-to-all | bytes 1245184 | tf_op jit(solution)/shard_map/all_to_all | solution.py:328
  173.1 2.7 %final_kernel.1 = (f32[64,128]{1,0:T(8,128)}, f32[64,128]{1,0:T(8,128)}, f32[16,128]{1,0:T(8,128)}) custom-call(bf16[16,152,128]{2,1,0:T(8,128)(2,1)} %all_to_all.16.in_ref), custom_call_target="tpu_custom_call" | custom-call | tf_op jit(solution)/shard_map/final_kernel/pallas_call | solution.py:330
Async XLA Ops:
  50.0 12.6 %copy-start.1 = (s32[128,1,48]{0,2,1:T(8,128)S(1)}, s32[128,1,48]{0,2,1:T(8,128)}, u32[]{:S(2)}) copy-start(s32[128,1,48]{0,2,1:T(8,128)} %param.17) | copy-start | bytes 73732
  53.3 31.3 %all-to-all-start = ((bf16[8,576,128]{2,1,0:T(8,128)(2,1)}), bf16[8,576,128]{2,1,0:T(8,128)(2,1)S(1)}, u32[]{:S(2)}, u32[]{:S(2)}) async-start(bf16[8,576,128]{2,1,0:T(8,128)(2,1)} %relay_kernel.1), calls=%async_computation | async-start | bytes 2359296 | tf_op jit(solution)/shard_map/all_to_all | solution.py:285
  84.6 1.0 copy-start

commit v4 on v2

--- a/solution.py
+++ b/solution.py
@@ -11,12 +11,14 @@
 TOPN = 12
 SUB = 4
 CMP = 32
-KV = ("kv_0", "kv_1")
+KV = ("kv_0", "kv_1", "kv_2")
+GROUP_AXES = KV[1:]
 FAR = 1 << 30
 WIDE = jnp.float32
 LOW = jnp.bfloat16
-SLOW = 16
-FAST = 8
+NEAR = 4
+SLOW = 16 // NEAR
+GROUP = 8 * NEAR
 PER = 4
 PAIR = 2 * DH
 ROWS = PER * BLK
@@ -33,26 +35,32 @@
     return lax.dot_general(a, b, (((ca,), (cb,)), ((), ())), preferred_element_type=WIDE)
 
 
-def pairs_kernel(keys_ref, values_ref, out_ref):
+def pairs_kernel(place_ref, keys_ref, values_ref, chosen_ref, out_ref, table_ref):
     both = jnp.concatenate([keys_ref[...], values_ref[...]], 0).astype(WIDE)
     out_ref[...] = both.T.astype(LOW)
-
-
-def relay_kernel(table_ref, all_ref, out_ref):
+    entry = chosen_ref[...]
+    own = place_ref[0] & (GROUP - 1)
+    owner = jnp.where(entry >= 0, entry // PER, -1)
+    inner = entry & (PER - 1)
+    for z in range(SLOW):
+        hit = jnp.where(owner == z * GROUP + own, inner, PER)
+        table_ref[z:z + 1, :] = jnp.min(hit, 0, keepdims=True)
+
+
+def relay_kernel(place_ref, table_ref, all_ref, out_ref):
+    column = place_ref[0] // GROUP * GROUP
     rows = all_ref[...].astype(WIDE).reshape(SLOW * PER, CMP, PAIR)
     means = jnp.mean(rows, 1).astype(LOW)
-    for y in range(FAST):
-        out_ref[y, SUMS:, :] = means
-
-    def one(z, carry):
-        for y in range(FAST):
-            at = (z * PER + jnp.minimum(table_ref[y * SLOW + z], PER - 1)) * BLK
-            out_ref[y, pl.ds(pl.multiple_of(z * BLK, BLK), BLK), :] = all_ref[
-                pl.ds(pl.multiple_of(at, BLK), BLK), :
-            ]
+
+    def one(g, carry):
+        out_ref[g, SUMS:, :] = means
+        for z in range(SLOW):
+            pick = jnp.minimum(table_ref[z, column + g], PER - 1)
+            at = pl.multiple_of((z * PER + pick) * BLK, BLK)
+            out_ref[g, z * BLK:(z + 1) * BLK, :] = all_ref[pl.ds(at, BLK), :]
         return carry
 
-    lax.fori_loop(0, SLOW, one, 0)
+    lax.fori_loop(0, GROUP, one, 0, unroll=2)
 
 
 def prep_kernel(q_ref, cot_ref, gates_ref, logs_ref, out_ref, msum_ref, msel_ref, ldsum_ref, ldsel_ref):
@@ -101,19 +109,19 @@
     m = msum_ref[...]
     ld = ldsum_ref[...]
     row_at = lax.broadcasted_iota(jnp.int32, (2 * ROWS, 1), 0) & (ROWS - 1)
-    per_fast = SLOW * PER
-    step = 4
-    lane = lax.broadcasted_iota(jnp.int32, (1, step * per_fast), 1)
+    per_one = SLOW * PER
+    step = 256 // per_one
+    lane = lax.broadcasted_iota(jnp.int32, (1, step * per_one), 1)
     dq_sum = jnp.zeros((2 * ROWS, PAIR), WIDE)
-    for y in range(0, FAST, step):
+    for y in range(0, GROUP, step):
         kv = jnp.concatenate([arr_ref[y + k, SUMS:, :] for k in range(step)], 0)
-        owner = (lane & (per_fast - 1)) // PER * FAST + y + lane // per_fast
+        owner = (lane & (per_one - 1)) // PER * GROUP + y + lane // per_one
         ends = (owner * PER + (lane & (PER - 1)) + 1) * CMP - 1 - base
         dq_part, kv_grad = grads(m, kv, ends <= row_at, ld)
         dq_sum += dq_part
         low = kv_grad.astype(LOW)
         for k in range(step):
-            ret_ref[y + k, SUMS:PARTS, :] = low[k * per_fast:(k + 1) * per_fast]
+            ret_ref[y + k, SUMS:PARTS, :] = low[k * per_one:(k + 1) * per_one]
     sub_at = lax.broadcasted_iota(jnp.int32, (2 * SUB_ROWS, 1), 0) & (SUB_ROWS - 1)
     sel_lane = lax.broadcasted_iota(jnp.int32, (1, TOPN * BLK), 1)
     for s in range(SUB):
@@ -123,8 +131,8 @@
             n = list_ref[s * TOPN + i]
             live = n >= 0
             owner = jnp.maximum(n, 0) // PER
-            fast = owner & (FAST - 1)
-            at = pl.multiple_of(owner // FAST * BLK, BLK)
+            fast = owner & (GROUP - 1)
+            at = pl.multiple_of(owner // GROUP * BLK, BLK)
             places.append((live, fast, at))
             kv_ref[i * BLK:(i + 1) * BLK, :] = arr_ref[fast, pl.ds(at, BLK), :]
             start = jnp.where(live, n * BLK - base - i * BLK, FAR)
@@ -147,35 +155,40 @@
             dq_ref[top:top + SUB_ROWS, h * DH:(h + 1) * DH] = total * scale
     load.wait()
     qb = dq_ref[...].astype(LOW)
-    span = FAST * COLS
+    span = GROUP * COLS
     for z in range(SLOW):
         part = dot(hid_here[:, z * span:(z + 1) * span], qb, 0, 0).astype(LOW)
-        for y in range(FAST):
+        for y in range(GROUP):
             ret_ref[y, PARTS + z * COLS:PARTS + (z + 1) * COLS, :] = part[y * COLS:(y + 1) * COLS]
 
 
-def merge_kernel(table_ref, in_ref, out_ref, tail_ref):
-    tail = in_ref[0, SUMS:PARTS, :].astype(WIDE)
-    for y in range(1, FAST):
-        tail = tail + in_ref[y, SUMS:PARTS, :].astype(WIDE)
-    tail_ref[:SLOW * PER, :] = tail
+def merge_kernel(place_ref, table_ref, in_ref, out_ref, tail_ref):
+    column = place_ref[0] // GROUP * GROUP
     tail_ref[SLOW * PER:, :] = jnp.zeros((8, PAIR), WIDE)
 
-    def one(z, carry):
-        sums = [jnp.zeros((BLK, PAIR), WIDE) for _ in range(PER)]
-        cols = jnp.zeros((COLS, PAIR), WIDE)
-        for y in range(FAST):
-            pick = table_ref[y * SLOW + z]
-            here = in_ref[y, pl.ds(pl.multiple_of(z * BLK, BLK), BLK), :].astype(WIDE)
-            sums = [sums[b] + jnp.where(pick == b, here, 0.0) for b in range(PER)]
-            cols = cols + in_ref[y, pl.ds(pl.multiple_of(PARTS + z * COLS, COLS), COLS), :].astype(WIDE)
+    def add_tail(g, tail):
+        return tail + in_ref[g, SUMS:PARTS, :].astype(WIDE)
+
+    tail_ref[:SLOW * PER, :] = lax.fori_loop(
+        0, GROUP, add_tail, jnp.zeros((SLOW * PER, PAIR), WIDE), unroll=8
+    )
+    for z in range(SLOW):
+
+        def one(g, carry, z=z):
+            sums, cols = carry
+            pick = table_ref[z, column + g]
+            here = in_ref[g, z * BLK:(z + 1) * BLK, :].astype(WIDE)
+            sums = tuple(sums[b] + jnp.where(pick == b, here, 0.0) for b in range(PER))
+            part = in_ref[g, PARTS + z * COLS:PARTS + (z + 1) * COLS, :]
+            return sums, cols + part.astype(WIDE)
+
+        zero = jnp.zeros((BLK, PAIR), WIDE)
+        start = ((zero,) * PER, jnp.zeros((COLS, PAIR), WIDE))
+        sums, cols = lax.fori_loop(0, GROUP, one, start, unroll=8)
         for b in range(PER):
             out_ref[z, b * BLK:(b + 1) * BLK, :] = sums[b].astype(LOW)
-        out_ref[z, ROWS:ROWS + 8, :] = tail_ref[pl.ds(z * PER, 8), :].astype(LOW)
+        out_ref[z, ROWS:ROWS + 8, :] = tail_ref[z * PER:z * PER + 8, :].astype(LOW)
         out_ref[z, ROWS + 8:, :] = cols.astype(LOW)
-        return carry
-
-    lax.fori_loop(0, SLOW, one, 0)
 
 
 def final_kernel(in_ref, gk_ref, gv_ref, gw_ref):
@@ -216,21 +229,19 @@
 
 
 def shards(queries, keys, values, hidden, log_sums, gates, branch_out, cotangent, chosen):
-    slow_at = lax.axis_index(KV[0])
-    fast_at = lax.axis_index(KV[1])
-    place = slow_at * FAST + fast_at
+    place = lax.axis_index(KV)
+    here = place[None]
     lists = chosen[:, 0]
-    near = lax.dynamic_slice_in_dim(lists, slow_at * FAST, FAST, 0)
-    owner = near // PER
-    ours = (near >= 0) & (owner % FAST == fast_at)
-    hits = ours[..., None] & ((owner // FAST)[..., None] == jnp.arange(SLOW, dtype=jnp.int32))
-    table = jnp.min(jnp.where(hits, (near % PER)[..., None], PER), 1).reshape(-1)
     listing = lax.dynamic_index_in_dim(lists, place, 0, keepdims=False)
 
-    pairs = call(pairs_kernel, [vmem(), vmem()], shape(ROWS, PAIR))(keys.T, values.T)
+    pairs, table = call(
+        pairs_kernel,
+        [smem(), vmem(), vmem(), vmem()],
+        (shape(ROWS, PAIR), shape(SLOW, lists.shape[0], kind=jnp.int32)),
+    )(here, keys.T, values.T, lists.T)
     along = lax.all_gather(pairs, KV[0], axis=0, tiled=True)
-    outbound = call(relay_kernel, [smem(), vmem()], shape(FAST, FETCH, PAIR))(table, along)
-    arrived = lax.all_to_all(outbound, KV[1], split_axis=0, concat_axis=0, tiled=True)
+    outbound = call(relay_kernel, [smem(), smem(), vmem()], shape(GROUP, FETCH, PAIR))(here, table, along)
+    arrived = lax.all_to_all(outbound, GROUP_AXES, split_axis=0, concat_axis=0, tiled=True)
 
     m_sum, m_sel, ld_sum, ld_sel = call(
         prep_kernel,
@@ -245,20 +256,20 @@
     grad_queries, returned = call(
         main_kernel,
         [smem(), smem()] + [vmem()] * 5 + [pl.BlockSpec(memory_space=pl.ANY)],
-        (shape(ROWS, PAIR, kind=WIDE), shape(FAST, BACK, PAIR)),
+        (shape(ROWS, PAIR, kind=WIDE), shape(GROUP, BACK, PAIR)),
         (
             pltpu.VMEM((TOPN * BLK, PAIR), LOW),
             pltpu.VMEM(hidden.shape, LOW),
             pltpu.SemaphoreType.DMA,
         ),
-    )(place[None], listing, m_sum, m_sel, ld_sum, ld_sel, arrived, hidden)
-    across = lax.all_to_all(returned, KV[1], split_axis=0, concat_axis=0, tiled=True)
+    )(here, listing, m_sum, m_sel, ld_sum, ld_sel, arrived, hidden)
+    across = lax.all_to_all(returned, GROUP_AXES, split_axis=0, concat_axis=0, tiled=True)
     merged = call(
         merge_kernel,
-        [smem(), vmem()],
+        [smem(), smem(), vmem()],
         shape(SLOW, LAST, PAIR),
         (pltpu.VMEM((SLOW * PER + 8, PAIR), WIDE),),
-    )(table, across)
+    )(here, table, across)
     home = lax.all_to_all(merged, KV[0], split_axis=0, concat_axis=0, tiled=True)
     turned_keys, turned_values, grad_weight = call(
         final_kernel,
@@ -269,7 +280,7 @@
 
 
 def solution(mesh):
-    finer = Mesh(mesh.devices.reshape(SLOW, FAST, mesh.shape["tp"]), ("kv_0", "kv_1", "tp"))
+    finer = Mesh(mesh.devices.reshape(SLOW, NEAR, 8, mesh.shape["tp"]), (*KV, "tp"))
     placed = (
         P(KV, "tp"),
         P(KV, "tp"),

time: 175 us -> 156 us (0.89)
  blocking collectives: 124 us -> 99.3 us
  waiting for transfers between devices: 21.3 us -> 25.5 us
  starting transfers between devices: 7.1 us -> 10.6 us
    all_gather x1, blocking collectives: 47.8 us -> 30.7 us  [shards(): along = lax.all_gather(pairs, KV[0], axis=0, tiled=True)]
    all_to_all x1, blocking collectives: 35.5 us -> 21.4 us  [shards(): lax.all_to_all(merged, KV[0], split_axis=0, concat_axis=0, tiled=True)]
    all_to_all x1, blocking collectives: 41 us -> 47.2 us  [shards(): lax.all_to_all(returned, GROUP_AXES, split_axis=0, concat_axis=0, tiled=T...]
    all_to_all x1, waiting for transfers between devices: 21.3 us -> 25.5 us  [shards(): lax.all_to_all(outbound, GROUP_AXES, split_axis=0, concat_axis=0, tiled=T...]
    all_to_all x1, starting transfers between devices: 7.1 us -> 10.6 us  [shards(): lax.all_to_all(outbound, GROUP_AXES, split_axis=0, concat_axis=0, tiled=T...]
where the time goes in v4:
time: 156 us; the launch traced here: 155 us
  blocking collectives  99.3 us (64%)
  waiting for transfers between devices  25.5 us (16%)
  Pallas kernels  16.9 us (11%)
  starting transfers between devices  10.6 us (7%)
  local copies, waits for them, and re-layouts  1.71 us (1%)
    all_to_all x1, blocking collectives, shards(): lax.all_to_all(returned, GROUP_AXES, split_axis=0, concat_axis=0, tiled=T...  47.2 us
    all_gather x1, blocking collectives, shards(): along = lax.all_gather(pairs, KV[0], axis=0, tiled=True)  30.7 us
    all_to_all x1, waiting for transfers between devices, shards(): lax.all_to_all(outbound, GROUP_AXES, split_axis=0, concat_axis=0, tiled=T...  25.5 us
    all_to_all x1, blocking collectives, shards(): lax.all_to_all(merged, KV[0], split_axis=0, concat_axis=0, tiled=True)  21.4 us
    all_to_all x1, starting transfers between devices, shards(): lax.all_to_all(outbound, GROUP_AXES, split_axis=0, concat_axis=0, tiled=T...  10.6 us
    pallas_call x1, Pallas kernels, shards(): call(main_kernel, [smem(), smem()] + [vmem()] * 5 + [pl.BlockSpec(memory_...  6.1 us
  transfers between devices with their start and end apart: 1, of which 1 were waited for; matrix products, arithmetic and copies ran while one was open for 0% of the time, Pallas kernels for 1%

profile of v4, /device:TPU:6, one launch (start us, length us, event | category | flops | bytes accessed | tf_op | source)
XLA Modules:
  0.0 154.7 jit_solution(13522465781208924339)
XLA Ops:
  0.6 1.5 pairs_kernel.1
  2.1 30.7 %all_gather.3.all_ref = bf16[512,128]{1,0:T(8,128)(2,1)} all-gather(bf16[128,128]{1,0:T(8,128)(2,1)} %get-tuple-element.20), channel_id=1, replica_groups=mesh['kv_0'=4,'kv_1'=4,'kv_2'=8,'tp'=8] {'kv_0'}, dimensions={0}, use_global_device_ids=true | all-gather | bytes 163840 | tf_op jit(solution)/shard_map/all_gather | solution.py:242
  32.8 0.0 copy-start.1
  32.8 2.4 %relay_kernel.1 = bf16[32,144,128]{2,1,0:T(8,128)(2,1)} custom-call(s32[1]{0:T(128)} %bitcast.place_ref, s32[4,128]{1,0:T(4,128)} %get-tuple-element.19.table_ref, bf16[512,128]{1,0:T(8,128)(2,1)} %all_gather.3.all_ref), custom_call_target="tpu_custom_call" | custom-call | tf_op jit(solution)/shard_map/relay_kernel/pallas_call | solution.py:243
  35.3 10.6 %all-to-all-start = ((bf16[32,144,128]{2,1,0:T(8,128)(2,1)}), bf16[32,144,128]{2,1,0:T(8,128)(2,1)S(1)}, u32[]{:S(2)}, u32[]{:S(2)}) async-start(bf16[32,144,128]{2,1,0:T(8,128)(2,1)} %relay_kernel.1), calls=%async_computation | async-start | bytes 2359296 | tf_op jit(solution)/shard_map/all_to_all | solution.py:244
  45.8 2.2 %prep_kernel.1 = (bf16[512,128]{1,0:T(8,128)(2,1)}, bf16[4,128,128]{2,1,0:T(8,128)(2,1)}, f32[256,2]{1,0:T(8,128)}, f32[4,64,2]{2,1,0:T(8,128)}) custom-call(bf16[128,128]{1,0:T(8,128)(2,1)} %q_ref.1, bf16[128,128]{1,0:T(8,128)(2,1)} %cot_ref.1, f32[2,2,128]{2,1,0:T(2,128)} %bitcast.13, f32[2,2,128]{2,1,0:T(2,128)} %bitcast.14, bf16[2,128,128]{2,1,0:T(8,128)(2,1)} %out_ref.1), custom_call_target="tpu_custom_call" | custom-call | tf_op jit(solution)/shard_map/prep_kernel/pallas_call | solution.py:246
  48.0 0.0 copy-done.1
  48.0 0.7 dynamic-slice_reduce_fusion.list_ref
  48.7 25.5 %all-to-all-done.arr_ref = bf16[32,144,128]{2,1,0:T(8,128)(2,1)S(1)} async-done(((bf16[32,144,128]{2,1,0:T(8,128)(2,1)}), bf16[32,144,128]{2,1,0:T(8,128)(2,1)S(1)}, u32[]{:S(2)}, u32[]{:S(2)}) %all-to-all-start) | async-done | bytes 1179680 | tf_op jit(solution)/shard_map/all_to_all | solution.py:244
  74.3 0.0 copy-start
  74.3 1.0 copy-done
  75.3 6.1 %main_kernel.1 = (f32[128,128]{1,0:T(8,128)}, bf16[32,208,128]{2,1,0:T(8,128)(2,1)}) custom-call(s32[1]{0:T(128)} %bitcast.place_ref, s32[48]{0:T(128)} %dynamic-slice_reduce_fusion.list_ref, bf16[512,128]{1,0:T(8,128)(2,1)} %get-tuple-element.15.msum_ref, bf16[4,128,128]{2,1,0:T(8,128)(2,1)} %get-tuple-element.16.msel_ref, ...), custom_call_target="tpu_custom_call" | custom-call | tf_op jit(solution)/shard_map/main_kernel/pallas_call | solution.py:256
  81.4 47.2 %all_to_all.15.in_ref = bf16[32,208,128]{2,1,0:T(8,128)(2,1)} all-to-all(bf16[32,208,128]{2,1,0:T(8,128)(2,1)} %get-tuple-element.22), channel_id=1, replica_groups=mesh['kv_0'=4,'kv_1'=4,'kv_2'=8,'tp'=8] {'kv_1','kv_2'}, dimensions={0} | all-to-all | bytes 3407872 | tf_op jit(solution)/shard_map/all_to_all | solution.py:266
  128.6 3.1 %merge_kernel.1 = bf16[4,152,128]{2,1,0:T(8,128)(2,1)} custom-call(s32[1]{0:T(128)} %bitcast.place_ref, s32[4,128]{1,0:T(4,128)} %get-tuple-element.19.table_ref, bf16[32,208,128]{2,1,0:T(8,128)(2,1)} %all_to_all.15.in_ref), custom_call_target="tpu_custom_call" | custom-call | tf_op jit(solution)/shard_map/merge_kernel/pallas_call | solution.py:267
  131.7 21.4 %all_to_all.16.in_ref = bf16[4,152,128]{2,1,0:T(8,128)(2,1)} all-to-all(bf16[4,152,128]{2,1,0:T(8,128)(2,1)} %merge_kernel.1), channel_id=1, replica_groups=mesh['kv_0'=4,'kv_1'=4,'kv_2'=8,'tp'=8] {'kv_0'}, dimensions={0} | all-to-all | bytes 311296 | tf_op jit(solution)/shard_map/all_to_all | solution.py:273
  153.1 1.6 %final_kernel.1 = (f32[64,128]{1,0:T(8,128)}, f32[64,128]{1,0:T(8,128)}, f32[16,128]{1,0:T(8,128)}) custom-call(bf16[4,152,128]{2,1,0:T(8,128)(2,1)} %all_to_all.16.in_ref), custom_call_target="tpu_custom_call" | custom-call | tf_op jit(solution)/shard_map/final_kernel/pallas_call | solution.py:274
Async XLA Ops:
  32.8 15.2 %copy-start.1 = (s32[128,1,48]{0,2,1:T(8,128)S(1)}, s32[128,1,48]{0,2,1:T(8,128)}, u32[]{:S(2)}) copy-start(s32[128,1,48]{0,2,1:T(8,128)} %param.17) | copy-start | bytes 73732
  35.3 39.0 %all-to-all-start = ((bf16[32,144,128]{2,1,0:T(8,128)(2,1)}), bf16[32,144,128]{2,1,0:T(8,128)(2,1)S(1)}, u32[]{:S(2)}, u32[]{:S(2)}) async-start(bf16[32,144,128]{2,1,0:T(8,128)(2,1)} %relay_kernel.1), calls=%async_computation | async-start | bytes 2359296 | tf_op jit(solution)/shard_map/all_to_all | solution.py:244
  74.3 1.0 copy-start

commit v5 on v4

--- a/solution.py
+++ b/solution.py
@@ -92,9 +92,7 @@
 
 
 def main_kernel(place_ref, list_ref, msum_ref, msel_ref, ldsum_ref, ldsel_ref, arr_ref, hid_ref,
-                dq_ref, ret_ref, kv_ref, hid_here, sem):
-    load = pltpu.make_async_copy(hid_ref, hid_here, sem)
-    load.start()
+                dq_ref, ret_ref, kv_ref):
     base = place_ref[0] * ROWS
     scale = DH ** (-0.5)
 
@@ -153,11 +151,10 @@
             total = dq_sum[h * ROWS + top:h * ROWS + top + SUB_ROWS, :DH]
             total = total + dq_part[h * SUB_ROWS:(h + 1) * SUB_ROWS, :DH]
             dq_ref[top:top + SUB_ROWS, h * DH:(h + 1) * DH] = total * scale
-    load.wait()
     qb = dq_ref[...].astype(LOW)
     span = GROUP * COLS
     for z in range(SLOW):
-        part = dot(hid_here[:, z * span:(z + 1) * span], qb, 0, 0).astype(LOW)
+        part = dot(hid_ref[:, z * span:(z + 1) * span], qb, 0, 0).astype(LOW)
         for y in range(GROUP):
             ret_ref[y, PARTS + z * COLS:PARTS + (z + 1) * COLS, :] = part[y * COLS:(y + 1) * COLS]
 
@@ -216,6 +213,14 @@
     return jax.ShapeDtypeStruct(sizes, kind)
 
 
+def local(*sizes, kind=LOW):
+    return pltpu.VMEM(sizes, kind)
+
+
+def inside(*arrays):
+    return [pltpu.with_memory_space_constraint(array, pltpu.VMEM) for array in arrays]
+
+
 def call(kernel, ins, outs, scratch=()):
     many = isinstance(outs, tuple)
     return pl.pallas_call(
@@ -224,6 +229,7 @@
         in_specs=ins,
         out_specs=tuple(vmem() for _ in outs) if many else vmem(),
         scratch_shapes=list(scratch),
+        compiler_params=pltpu.CompilerParams(vmem_limit_bytes=16 << 20),
         name=kernel.__name__,
     )
 
@@ -237,45 +243,41 @@
     pairs, table = call(
         pairs_kernel,
         [smem(), vmem(), vmem(), vmem()],
-        (shape(ROWS, PAIR), shape(SLOW, lists.shape[0], kind=jnp.int32)),
+        (local(ROWS, PAIR), shape(SLOW, lists.shape[0], kind=jnp.int32)),
     )(here, keys.T, values.T, lists.T)
     along = lax.all_gather(pairs, KV[0], axis=0, tiled=True)
-    outbound = call(relay_kernel, [smem(), smem(), vmem()], shape(GROUP, FETCH, PAIR))(here, table, along)
+    outbound = call(relay_kernel, [smem(), smem(), vmem()], local(GROUP, FETCH, PAIR))(here, table, *inside(along))
     arrived = lax.all_to_all(outbound, GROUP_AXES, split_axis=0, concat_axis=0, tiled=True)
 
     m_sum, m_sel, ld_sum, ld_sel = call(
         prep_kernel,
         [vmem()] * 5,
         (
-            shape(4 * ROWS, PAIR),
-            shape(SUB, 4 * SUB_ROWS, PAIR),
-            shape(2 * ROWS, 2, kind=WIDE),
-            shape(SUB, 2 * SUB_ROWS, 2, kind=WIDE),
+            local(4 * ROWS, PAIR),
+            local(SUB, 4 * SUB_ROWS, PAIR),
+            local(2 * ROWS, 2, kind=WIDE),
+            local(SUB, 2 * SUB_ROWS, 2, kind=WIDE),
         ),
     )(queries, cotangent, jnp.transpose(gates, (0, 2, 1)), jnp.transpose(log_sums, (0, 2, 1)), branch_out)
     grad_queries, returned = call(
         main_kernel,
-        [smem(), smem()] + [vmem()] * 5 + [pl.BlockSpec(memory_space=pl.ANY)],
-        (shape(ROWS, PAIR, kind=WIDE), shape(GROUP, BACK, PAIR)),
-        (
-            pltpu.VMEM((TOPN * BLK, PAIR), LOW),
-            pltpu.VMEM(hidden.shape, LOW),
-            pltpu.SemaphoreType.DMA,
-        ),
-    )(here, listing, m_sum, m_sel, ld_sum, ld_sel, arrived, hidden)
+        [smem(), smem()] + [vmem()] * 6,
+        (shape(ROWS, PAIR, kind=WIDE), local(GROUP, BACK, PAIR)),
+        (pltpu.VMEM((TOPN * BLK, PAIR), LOW),),
+    )(here, listing, *inside(m_sum, m_sel, ld_sum, ld_sel, arrived, hidden))
     across = lax.all_to_all(returned, GROUP_AXES, split_axis=0, concat_axis=0, tiled=True)
     merged = call(
         merge_kernel,
         [smem(), smem(), vmem()],
-        shape(SLOW, LAST, PAIR),
+        local(SLOW, LAST, PAIR),
         (pltpu.VMEM((SLOW * PER + 8, PAIR), WIDE),),
-    )(here, table, across)
+    )(here, table, *inside(across))
     home = lax.all_to_all(merged, KV[0], split_axis=0, concat_axis=0, tiled=True)
     turned_keys, turned_values, grad_weight = call(
         final_kernel,
         [vmem()],
         (shape(DH, ROWS, kind=WIDE), shape(DH, ROWS, kind=WIDE), shape(COLS, PAIR, kind=WIDE)),
-    )(home)
+    )(*inside(home))
     return (grad_queries, turned_keys.T, turned_values.T, grad_weight)
 
 

time: 156 us -> 151 us (0.968)
  Pallas kernels: 16.9 us -> 9.23 us
  waiting for transfers between devices: 25.5 us -> 27.3 us
    pallas_call x5, Pallas kernels: 15.3 us -> 8.51 us  [the longest x1 4.19 us: shards(): call(main_kernel, [smem(), smem()] + [vmem()] * 6, (shape(ROWS, PAIR, kin...]
    all_to_all x1, waiting for transfers between devices: 25.5 us -> 27.3 us  [shards(): lax.all_to_all(outbound, GROUP_AXES, split_axis=0, concat_axis=0, tiled=T...]
  transfers between devices with their start and end apart: 1 -> 1, of which waited for: 1 -> 1; matrix products, arithmetic and copies ran while one was open for 0% -> 0% of each run, Pallas kernels for 1% -> 0%
where the time goes in v5:
time: 151 us; the launch traced here: 149 us
  blocking collectives  98.3 us (65%)
  waiting for transfers between devices  27.3 us (18%)
  starting transfers between devices  10.8 us (7%)
  Pallas kernels  9.23 us (6%)
  local copies, waits for them, and re-layouts  2.38 us (2%)
    all_to_all x1, blocking collectives, shards(): lax.all_to_all(returned, GROUP_AXES, split_axis=0, concat_axis=0, tiled=T...  47.5 us
    all_gather x1, blocking collectives, shards(): along = lax.all_gather(pairs, KV[0], axis=0, tiled=True)  29.7 us
    all_to_all x1, waiting for transfers between devices, shards(): lax.all_to_all(outbound, GROUP_AXES, split_axis=0, concat_axis=0, tiled=T...  27.3 us
    all_to_all x1, blocking collectives, shards(): lax.all_to_all(merged, KV[0], split_axis=0, concat_axis=0, tiled=True)  21.2 us
    all_to_all x1, starting transfers between devices, shards(): lax.all_to_all(outbound, GROUP_AXES, split_axis=0, concat_axis=0, tiled=T...  10.8 us
    pallas_call x1, Pallas kernels, shards(): call(main_kernel, [smem(), smem()] + [vmem()] * 6, (shape(ROWS, PAIR, kin...  4.19 us
  transfers between devices with their start and end apart: 1, of which 1 were waited for; matrix products, arithmetic and copies ran while one was open for 0% of the time, Pallas kernels for 0%

profile of v5, /device:TPU:6, one launch (start us, length us, event | category | flops | bytes accessed | tf_op | source)
XLA Modules:
  0.0 148.7 jit_solution(6490658756694173623)
XLA Ops:
  0.6 0.0 copy-start.1
  0.7 0.7 copy-done.1
  1.4 0.0 copy-start.6
  1.4 0.7 copy-done.6
  2.1 0.0 copy-start.7
  2.1 0.7 copy-done.7
  2.8 0.1 pairs_kernel.1
  2.9 29.7 %all_gather.3.all_ref = bf16[512,128]{1,0:T(8,128)(2,1)S(1)} all-gather(bf16[128,128]{1,0:T(8,128)(2,1)S(1)} %get-tuple-element.20), channel_id=1, replica_groups=mesh['kv_0'=4,'kv_1'=4,'kv_2'=8,'tp'=8] {'kv_0'}, dimensions={0}, use_global_device_ids=true | all-gather | bytes 163840 | tf_op jit(solution)/shard_map/all_gather | solution.py:248
  32.6 0.0 copy-start.3
  32.6 0.0 copy-start.4
  32.6 0.0 copy-start.5
  32.6 0.0 copy-start.8
  32.6 0.0 copy-start.9
  32.6 0.0 copy-start.2
  32.6 0.0 copy-start
  32.6 2.1 %relay_kernel.1 = bf16[32,144,128]{2,1,0:T(8,128)(2,1)} custom-call(s32[1]{0:T(128)} %bitcast.place_ref, s32[4,128]{1,0:T(4,128)S(1)} %get-tuple-element.19.table_ref, bf16[512,128]{1,0:T(8,128)(2,1)S(1)} %all_gather.3.all_ref), custom_call_target="tpu_custom_call" | custom-call | tf_op jit(solution)/shard_map/relay_kernel/pallas_call | solution.py:249
  34.7 10.8 %all-to-all-start = ((bf16[32,144,128]{2,1,0:T(8,128)(2,1)}), bf16[32,144,128]{2,1,0:T(8,128)(2,1)S(1)}, u32[]{:S(2)}, u32[]{:S(2)}) async-start(bf16[32,144,128]{2,1,0:T(8,128)(2,1)} %relay_kernel.1), calls=%async_computation | async-start | bytes 2359296 | tf_op jit(solution)/shard_map/all_to_all | solution.py:250
  45.5 0.0 copy-done.3
  45.5 0.0 copy-done.4
  45.5 0.0 copy-done.5
  45.5 0.0 copy-done.8
  45.5 0.0 copy-done.9
  45.5 0.6 prep_kernel.1
  46.1 0.0 copy-done.2
  46.1 0.2 dynamic-slice_reduce_fusion.list_ref
  46.3 27.3 %all-to-all-done.arr_ref = bf16[32,144,128]{2,1,0:T(8,128)(2,1)S(1)} async-done(((bf16[32,144,128]{2,1,0:T(8,128)(2,1)}), bf16[32,144,128]{2,1,0:T(8,128)(2,1)S(1)}, u32[]{:S(2)}, u32[]{:S(2)}) %all-to-all-start) | async-done | bytes 1179680 | tf_op jit(solution)/shard_map/all_to_all | solution.py:250
  73.6 0.0 copy-done
  73.6 4.2 %main_kernel.1 = (f32[128,128]{1,0:T(8,128)}, bf16[32,208,128]{2,1,0:T(8,128)(2,1)S(1)}) custom-call(s32[1]{0:T(128)} %bitcast.place_ref, s32[48]{0:T(128)S(1)} %dynamic-slice_reduce_fusion.list_ref, bf16[512,128]{1,0:T(8,128)(2,1)S(1)} %get-tuple-element.15.msum_ref, bf16[4,128,128]{2,1,0:T(8,128)(2,1)S(1)} %get-tuple-element.16.msel_ref, ...), custom_call_target="tpu_custom_call" | custom-call | tf_op jit(solution)/shard_map/main_kernel/pallas_call | solution.py:262
  77.8 47.5 %all_to_all.15.in_ref = bf16[32,208,128]{2,1,0:T(8,128)(2,1)S(1)} all-to-all(bf16[32,208,128]{2,1,0:T(8,128)(2,1)S(1)} %get-tuple-element.22), channel_id=1, replica_groups=mesh['kv_0'=4,'kv_1'=4,'kv_2'=8,'tp'=8] {'kv_1','kv_2'}, dimensions={0} | all-to-all | bytes 3407872 | tf_op jit(solution)/shard_map/all_to_all | solution.py:268
  125.3 1.6 %merge_kernel.1 = bf16[4,152,128]{2,1,0:T(8,128)(2,1)S(1)} custom-call(s32[1]{0:T(128)} %bitcast.place_ref, s32[4,128]{1,0:T(4,128)S(1)} %get-tuple-element.19.table_ref, bf16[32,208,128]{2,1,0:T(8,128)(2,1)S(1)} %all_to_all.15.in_ref), custom_call_target="tpu_custom_call" | custom-call | tf_op jit(solution)/shard_map/merge_kernel/pallas_call | solution.py:269
  126.9 21.2 %all_to_all.16.in_ref = bf16[4,152,128]{2,1,0:T(8,128)(2,1)S(1)} all-to-all(bf16[4,152,128]{2,1,0:T(8,128)(2,1)S(1)} %merge_kernel.1), channel_id=1, replica_groups=mesh['kv_0'=4,'kv_1'=4,'kv_2'=8,'tp'=8] {'kv_0'}, dimensions={0} | all-to-all | bytes 311296 | tf_op jit(solution)/shard_map/all_to_all | solution.py:275
  148.0 0.7 final_kernel.1
Async XLA Ops:
  0.6 0.7 copy-start.1
  1.4 0.7 copy-start.6
  2.1 0.7 copy-start.7
  32.6 12.9 %copy-start.3 = (bf16[2,128,128]{2,1,0:T(8,128)(2,1)S(1)}, bf16[2,128,128]{2,1,0:T(8,128)(2,1)}, u32[]{:S(2)}) copy-start(bf16[2,128,128]{2,1,0:T(8,128)(2,1)} %out_ref.1) | copy-start | bytes 196612
  32.6 12.9 %copy-start.4 = (bf16[128,128]{1,0:T(8,128)(2,1)S(1)}, bf16[128,128]{1,0:T(8,128)(2,1)}, u32[]{:S(2)}) copy-start(bf16[128,128]{1,0:T(8,128)(2,1)} %q_ref.1) | copy-start | bytes 98308
  32.6 12.9 %copy-start.5 = (bf16[128,128]{1,0:T(8,128)(2,1)S(1)}, bf16[128,128]{1,0:T(8,128)(2,1)}, u32[]{:S(2)}) copy-start(bf16[128,128]{1,0:T(8,128)(2,1)} %cot_ref.1) | copy-start | bytes 98308
  32.6 12.9 %copy-start.8 = (f32[2,128,2]{1,2,0:T(2,128)S(1)}, f32[2,128,2]{1,2,0:T(2,128)}, u32[]{:S(2)}) copy-start(f32[2,128,2]{1,2,0:T(2,128)} %param.14) | copy-start | bytes 6148
  32.6 12.9 %copy-start.9 = (f32[2,128,2]{1,2,0:T(2,128)S(1)}, f32[2,128,2]{1,2,0:T(2,128)}, u32[]{:S(2)}) copy-start(f32[2,128,2]{1,2,0:T(2,128)} %param.13) | copy-start | bytes 6148
  32.6 13.5 %copy-start.2 = (s32[128,1,48]{0,2,1:T(8,128)S(1)}, s32[128,1,48]{0,2,1:T(8,128)}, u32[]{:S(2)}) copy-start(s32[128,1,48]{0,2,1:T(8,128)} %param.17) | copy-start | bytes 73732
  32.6 41.0 %copy-start = (bf16[128,2048]{1,0:T(8,128)(2,1)S(1)}, bf16[128,2048]{1,0:T(8,128)(2,1)}, u32[]{:S(2)}) copy-start(bf16[128,2048]{1,0:T(8,128)(2,1)} %hid_ref.1) | copy-start | bytes 1572868
  34.7 38.9 %all-to-all-start = ((bf16[32,144,128]{2,1,0:T(8,128)(2,1)}), bf16[32,144,128]{2,1,0:T(8,128)(2,1)S(1)}, u32[]{:S(2)}, u32[]{:S(2)}) async-start(bf16[32,144,128]{2,1,0:T(8,128)(2,1)} %relay_kernel.1), calls=%async_computation | async-start | bytes 2359296 | tf_op jit(solution)/shard_map/all_to_all | solution.py:250

commit v6 on v5

--- a/solution.py
+++ b/solution.py
@@ -16,7 +16,7 @@
 FAR = 1 << 30
 WIDE = jnp.float32
 LOW = jnp.bfloat16
-NEAR = 4
+NEAR = 2
 SLOW = 16 // NEAR
 GROUP = 8 * NEAR
 PER = 4
@@ -35,10 +35,12 @@
     return lax.dot_general(a, b, (((ca,), (cb,)), ((), ())), preferred_element_type=WIDE)
 
 
-def pairs_kernel(place_ref, keys_ref, values_ref, chosen_ref, out_ref, table_ref):
+def pairs_kernel(place_ref, keys_ref, values_ref, chosen_ref, out_ref, table_ref, list_ref, turned_ref):
     both = jnp.concatenate([keys_ref[...], values_ref[...]], 0).astype(WIDE)
     out_ref[...] = both.T.astype(LOW)
     entry = chosen_ref[...]
+    turned_ref[...] = entry.T
+    list_ref[...] = turned_ref[pl.ds(place_ref[0], 1), :]
     own = place_ref[0] & (GROUP - 1)
     owner = jnp.where(entry >= 0, entry // PER, -1)
     inner = entry & (PER - 1)
@@ -126,7 +128,7 @@
         at_key = jnp.full((1, TOPN * BLK), FAR, jnp.int32)
         places = []
         for i in range(TOPN):
-            n = list_ref[s * TOPN + i]
+            n = list_ref[0, s * TOPN + i]
             live = n >= 0
             owner = jnp.maximum(n, 0) // PER
             fast = owner & (GROUP - 1)
@@ -238,17 +240,21 @@
     place = lax.axis_index(KV)
     here = place[None]
     lists = chosen[:, 0]
-    listing = lax.dynamic_index_in_dim(lists, place, 0, keepdims=False)
-
-    pairs, table = call(
+    pairs, table, listing = call(
         pairs_kernel,
         [smem(), vmem(), vmem(), vmem()],
-        (local(ROWS, PAIR), shape(SLOW, lists.shape[0], kind=jnp.int32)),
-    )(here, keys.T, values.T, lists.T)
+        (
+            local(ROWS, PAIR),
+            shape(SLOW, lists.shape[0], kind=jnp.int32),
+            shape(1, lists.shape[1], kind=jnp.int32),
+        ),
+        (pltpu.VMEM(lists.shape, jnp.int32),),
+    )(here, *[pltpu.with_memory_space_constraint(array, pltpu.HBM) for array in (keys.T, values.T, lists.T)])
     along = lax.all_gather(pairs, KV[0], axis=0, tiled=True)
     outbound = call(relay_kernel, [smem(), smem(), vmem()], local(GROUP, FETCH, PAIR))(here, table, *inside(along))
     arrived = lax.all_to_all(outbound, GROUP_AXES, split_axis=0, concat_axis=0, tiled=True)
 
+    arrived, queries = lax.optimization_barrier((arrived, queries))
     m_sum, m_sel, ld_sum, ld_sel = call(
         prep_kernel,
         [vmem()] * 5,

time: 151 us -> 159 us (1.053); the launches traced: 149 us -> 159 us
  blocking collectives: 98.3 us -> 149 us
  waiting for transfers between devices: 27.3 us -> 0 us
  starting transfers between devices: 10.8 us -> 0 us
  local copies, waits for them, and re-layouts: 2.38 us -> 0.03 us
    all_to_all x0 -> x1, blocking collectives: none -> 33 us  [shards(): lax.all_to_all(outbound, GROUP_AXES, split_axis=0, concat_axis=0, tiled=T...]
    all_to_all x1 -> x0, waiting for transfers between devices: 27.3 us -> none  [shards(): lax.all_to_all(outbound, GROUP_AXES, split_axis=0, concat_axis=0, tiled=T...]
    all_gather x1, blocking collectives: 29.7 us -> 41.2 us  [shards(): along = lax.all_gather(pairs, KV[0], axis=0, tiled=True)]
    all_to_all x1 -> x0, starting transfers between devices: 10.8 us -> none  [shards(): lax.all_to_all(outbound, GROUP_AXES, split_axis=0, concat_axis=0, tiled=T...]
    all_to_all x1, blocking collectives: 21.2 us -> 30 us  [shards(): lax.all_to_all(merged, KV[0], split_axis=0, concat_axis=0, tiled=True)]
    all_to_all x1, blocking collectives: 47.5 us -> 45 us  [shards(): lax.all_to_all(returned, GROUP_AXES, split_axis=0, concat_axis=0, tiled=T...]
    unnamed x20 -> x12, local copies, waits for them, and re-layouts: 2.2 us -> 0.03 us
  transfers between devices with their start and end apart: 1 -> 0, of which waited for: 1 -> 0; matrix products, arithmetic and copies ran while one was open for 0% -> 0% of each run, Pallas kernels for 0% -> 0%
where the time goes in v6:
time: 159 us
  blocking collectives  149 us (94%)
  Pallas kernels  9.08 us (6%)
    all_to_all x1, blocking collectives, shards(): lax.all_to_all(returned, GROUP_AXES, split_axis=0, concat_axis=0, tiled=T...  45 us
    all_gather x1, blocking collectives, shards(): along = lax.all_gather(pairs, KV[0], axis=0, tiled=True)  41.2 us
    all_to_all x1, blocking collectives, shards(): lax.all_to_all(outbound, GROUP_AXES, split_axis=0, concat_axis=0, tiled=T...  33 us
    all_to_all x1, blocking collectives, shards(): lax.all_to_all(merged, KV[0], split_axis=0, concat_axis=0, tiled=True)  30 us
    pallas_call x1, Pallas kernels, shards(): call(main_kernel, [smem(), smem()] + [vmem()] * 6, (shape(ROWS, PAIR, kin...  4.2 us

profile of v6, /device:TPU:6, one launch (start us, length us, event | category | flops | bytes accessed | tf_op | source)
XLA Modules:
  0.0 159.0 jit_solution(6095116495232409880)
XLA Ops:
  0.6 0.9 pairs_kernel.1
  1.5 41.2 %all_gather.3.all_ref = bf16[1024,128]{1,0:T(8,128)(2,1)S(1)} all-gather(bf16[128,128]{1,0:T(8,128)(2,1)S(1)} %get-tuple-element.20), channel_id=1, replica_groups=mesh['kv_0'=8,'kv_1'=2,'kv_2'=8,'tp'=8] {'kv_0'}, dimensions={0}, use_global_device_ids=true | all-gather | bytes 294912 | tf_op jit(solution)/shard_map/all_gather | solution.py:253
  42.7 0.0 copy-start.1
  42.7 0.0 copy-start.2
  42.8 0.0 copy-start.3
  42.8 0.0 copy-start.4
  42.8 0.0 copy-start.5
  42.8 0.0 copy-start
  42.8 1.1 relay_kernel.1
  43.9 33.0 %all_to_all.15.arr_ref = bf16[16,288,128]{2,1,0:T(8,128)(2,1)S(1)} all-to-all(bf16[16,288,128]{2,1,0:T(8,128)(2,1)S(1)} %relay_kernel.1), channel_id=1, replica_groups=mesh['kv_0'=8,'kv_1'=2,'kv_2'=8,'tp'=8] {'kv_1','kv_2'}, dimensions={0} | all-to-all | bytes 2359296 | tf_op jit(solution)/shard_map/all_to_all | solution.py:255
  76.9 0.0 copy-done.1
  76.9 0.0 copy-done.2
  76.9 0.0 copy-done.3
  76.9 0.0 copy-done.4
  76.9 0.0 copy-done.5
  76.9 0.6 prep_kernel.1
  77.5 0.0 copy-done
  77.5 4.2 %main_kernel.1 = (f32[128,128]{1,0:T(8,128)}, bf16[16,416,128]{2,1,0:T(8,128)(2,1)S(1)}) custom-call(s32[1]{0:T(128)} %bitcast.place_ref, s32[1,48]{1,0:T(1,128)S(1)} %get-tuple-element.18.list_ref, bf16[512,128]{1,0:T(8,128)(2,1)S(1)} %get-tuple-element.22.msum_ref, bf16[4,128,128]{2,1,0:T(8,128)(2,1)S(1)} %get-tuple-element.23.msel_ref, ...), custom_call_target="tpu_custom_call" | custom-call | tf_op jit(solution)/shard_map/main_kernel/pallas_call | solution.py:268
  81.8 45.0 %all_to_all.16.in_ref = bf16[16,416,128]{2,1,0:T(8,128)(2,1)S(1)} all-to-all(bf16[16,416,128]{2,1,0:T(8,128)(2,1)S(1)} %get-tuple-element.28), channel_id=1, replica_groups=mesh['kv_0'=8,'kv_1'=2,'kv_2'=8,'tp'=8] {'kv_1','kv_2'}, dimensions={0} | all-to-all | bytes 3407872 | tf_op jit(solution)/shard_map/all_to_all | solution.py:274
  126.8 1.6 merge_kernel.1
  128.3 30.0 %all_to_all.17.in_ref = bf16[8,152,128]{2,1,0:T(8,128)(2,1)S(1)} all-to-all(bf16[8,152,128]{2,1,0:T(8,128)(2,1)S(1)} %merge_kernel.1), channel_id=1, replica_groups=mesh['kv_0'=8,'kv_1'=2,'kv_2'=8,'tp'=8] {'kv_0'}, dimensions={0} | all-to-all | bytes 622592 | tf_op jit(solution)/shard_map/all_to_all | solution.py:281
  158.3 0.7 final_kernel.1
Async XLA Ops:
  42.7 34.2 %copy-start.1 = (bf16[2,128,128]{2,1,0:T(8,128)(2,1)S(1)}, bf16[2,128,128]{2,1,0:T(8,128)(2,1)}, u32[]{:S(2)}) copy-start(bf16[2,128,128]{2,1,0:T(8,128)(2,1)} %out_ref.1) | copy-start | bytes 196612
  42.7 34.2 %copy-start.2 = (bf16[128,128]{1,0:T(8,128)(2,1)S(1)}, bf16[128,128]{1,0:T(8,128)(2,1)}, u32[]{:S(2)}) copy-start(bf16[128,128]{1,0:T(8,128)(2,1)} %q_ref) | copy-start | bytes 98308
  42.8 34.2 %copy-start.3 = (bf16[128,128]{1,0:T(8,128)(2,1)S(1)}, bf16[128,128]{1,0:T(8,128)(2,1)}, u32[]{:S(2)}) copy-start(bf16[128,128]{1,0:T(8,128)(2,1)} %cot_ref.1) | copy-start | bytes 98308
  42.8 34.2 %copy-start.4 = (f32[2,128,2]{1,2,0:T(2,128)S(1)}, f32[2,128,2]{1,2,0:T(2,128)}, u32[]{:S(2)}) copy-start(f32[2,128,2]{1,2,0:T(2,128)} %param.14) | copy-start | bytes 6148
  42.8 34.2 %copy-start.5 = (f32[2,128,2]{1,2,0:T(2,128)S(1)}, f32[2,128,2]{1,2,0:T(2,128)}, u32[]{:S(2)}) copy-start(f32[2,128,2]{1,2,0:T(2,128)} %param.13) | copy-start | bytes 6148
  42.8 34.8 %copy-start = (bf16[128,2048]{1,0:T(8,128)(2,1)S(1)}, bf16[128,2048]{1,0:T(8,128)(2,1)}, u32[]{:S(2)}) copy-start(bf16[128,2048]{1,0:T(8,128)(2,1)} %hid_ref.1) | copy-start | bytes 1572868

commit v7 on v6

--- a/solution.py
+++ b/solution.py
@@ -16,7 +16,7 @@
 FAR = 1 << 30
 WIDE = jnp.float32
 LOW = jnp.bfloat16
-NEAR = 2
+NEAR = 4
 SLOW = 16 // NEAR
 GROUP = 8 * NEAR
 PER = 4

time: 159 us -> 148 us (0.931)
  blocking collectives: 149 us -> 138 us
    all_gather x1, blocking collectives: 41.2 us -> 29.7 us  [shards(): along = lax.all_gather(pairs, KV[0], axis=0, tiled=True)]
    all_to_all x1, blocking collectives: 33 us -> 40.8 us  [shards(): lax.all_to_all(outbound, GROUP_AXES, split_axis=0, concat_axis=0, tiled=T...]
    all_to_all x1, blocking collectives: 30 us -> 22.5 us  [shards(): lax.all_to_all(merged, KV[0], split_axis=0, concat_axis=0, tiled=True)]
where the time goes in v7:
time: 148 us
  blocking collectives  138 us (93%)
  Pallas kernels  8.99 us (6%)
    all_to_all x1, blocking collectives, shards(): lax.all_to_all(returned, GROUP_AXES, split_axis=0, concat_axis=0, tiled=T...  44.9 us
    all_to_all x1, blocking collectives, shards(): lax.all_to_all(outbound, GROUP_AXES, split_axis=0, concat_axis=0, tiled=T...  40.8 us
    all_gather x1, blocking collectives, shards(): along = lax.all_gather(pairs, KV[0], axis=0, tiled=True)  29.7 us
    all_to_all x1, blocking collectives, shards(): lax.all_to_all(merged, KV[0], split_axis=0, concat_axis=0, tiled=True)  22.5 us
    pallas_call x1, Pallas kernels, shards(): call(main_kernel, [smem(), smem()] + [vmem()] * 6, (shape(ROWS, PAIR, kin...  4.2 us

profile of v7, /device:TPU:6, one launch (start us, length us, event | category | flops | bytes accessed | tf_op | source)
XLA Modules:
  0.0 147.6 jit_solution(7474144681881354924)
XLA Ops:
  0.6 0.9 pairs_kernel.1
  1.5 29.7 %all_gather.3.all_ref = bf16[512,128]{1,0:T(8,128)(2,1)S(1)} all-gather(bf16[128,128]{1,0:T(8,128)(2,1)S(1)} %get-tuple-element.20), channel_id=1, replica_groups=mesh['kv_0'=4,'kv_1'=4,'kv_2'=8,'tp'=8] {'kv_0'}, dimensions={0}, use_global_device_ids=true | all-gather | bytes 163840 | tf_op jit(solution)/shard_map/all_gather | solution.py:253
  31.2 0.0 copy-start.1
  31.2 0.0 copy-start.2
  31.2 0.0 copy-start.3
  31.2 0.0 copy-start.4
  31.2 0.0 copy-start.5
  31.2 0.0 copy-start
  31.2 1.0 relay_kernel.1
  32.3 40.8 %all_to_all.15.arr_ref = bf16[32,144,128]{2,1,0:T(8,128)(2,1)S(1)} all-to-all(bf16[32,144,128]{2,1,0:T(8,128)(2,1)S(1)} %relay_kernel.1), channel_id=1, replica_groups=mesh['kv_0'=4,'kv_1'=4,'kv_2'=8,'tp'=8] {'kv_1','kv_2'}, dimensions={0} | all-to-all | bytes 2359296 | tf_op jit(solution)/shard_map/all_to_all | solution.py:255
  73.1 0.0 copy-done.1
  73.1 0.0 copy-done.2
  73.1 0.0 copy-done.3
  73.1 0.0 copy-done.4
  73.1 0.0 copy-done.5
  73.1 0.6 prep_kernel.1
  73.7 0.0 copy-done
  73.7 4.2 %main_kernel.1 = (f32[128,128]{1,0:T(8,128)}, bf16[32,208,128]{2,1,0:T(8,128)(2,1)S(1)}) custom-call(s32[1]{0:T(128)} %bitcast.place_ref, s32[1,48]{1,0:T(1,128)S(1)} %get-tuple-element.18.list_ref, bf16[512,128]{1,0:T(8,128)(2,1)S(1)} %get-tuple-element.22.msum_ref, bf16[4,128,128]{2,1,0:T(8,128)(2,1)S(1)} %get-tuple-element.23.msel_ref, ...), custom_call_target="tpu_custom_call" | custom-call | tf_op jit(solution)/shard_map/main_kernel/pallas_call | solution.py:268
  77.9 44.9 %all_to_all.16.in_ref = bf16[32,208,128]{2,1,0:T(8,128)(2,1)S(1)} all-to-all(bf16[32,208,128]{2,1,0:T(8,128)(2,1)S(1)} %get-tuple-element.28), channel_id=1, replica_groups=mesh['kv_0'=4,'kv_1'=4,'kv_2'=8,'tp'=8] {'kv_1','kv_2'}, dimensions={0} | all-to-all | bytes 3407872 | tf_op jit(solution)/shard_map/all_to_all | solution.py:274
  122.8 1.6 %merge_kernel.1 = bf16[4,152,128]{2,1,0:T(8,128)(2,1)S(1)} custom-call(s32[1]{0:T(128)} %bitcast.place_ref, s32[4,128]{1,0:T(4,128)S(1)} %get-tuple-element.19.table_ref, bf16[32,208,128]{2,1,0:T(8,128)(2,1)S(1)} %all_to_all.16.in_ref), custom_call_target="tpu_custom_call" | custom-call | tf_op jit(solution)/shard_map/merge_kernel/pallas_call | solution.py:275
  124.4 22.5 %all_to_all.17.in_ref = bf16[4,152,128]{2,1,0:T(8,128)(2,1)S(1)} all-to-all(bf16[4,152,128]{2,1,0:T(8,128)(2,1)S(1)} %merge_kernel.1), channel_id=1, replica_groups=mesh['kv_0'=4,'kv_1'=4,'kv_2'=8,'tp'=8] {'kv_0'}, dimensions={0} | all-to-all | bytes 311296 | tf_op jit(solution)/shard_map/all_to_all | solution.py:281
  146.8 0.7 final_kernel.1
Async XLA Ops:
  31.2 41.9 %copy-start.1 = (bf16[2,128,128]{2,1,0:T(8,128)(2,1)S(1)}, bf16[2,128,128]{2,1,0:T(8,128)(2,1)}, u32[]{:S(2)}) copy-start(bf16[2,128,128]{2,1,0:T(8,128)(2,1)} %out_ref.1) | copy-start | bytes 196612
  31.2 41.9 %copy-start.2 = (bf16[128,128]{1,0:T(8,128)(2,1)S(1)}, bf16[128,128]{1,0:T(8,128)(2,1)}, u32[]{:S(2)}) copy-start(bf16[128,128]{1,0:T(8,128)(2,1)} %q_ref) | copy-start | bytes 98308
  31.2 41.9 %copy-start.3 = (bf16[128,128]{1,0:T(8,128)(2,1)S(1)}, bf16[128,128]{1,0:T(8,128)(2,1)}, u32[]{:S(2)}) copy-start(bf16[128,128]{1,0:T(8,128)(2,1)} %cot_ref.1) | copy-start | bytes 98308
  31.2 41.9 %copy-start.4 = (f32[2,128,2]{1,2,0:T(2,128)S(1)}, f32[2,128,2]{1,2,0:T(2,128)}, u32[]{:S(2)}) copy-start(f32[2,128,2]{1,2,0:T(2,128)} %param.14) | copy-start | bytes 6148
  31.2 41.9 %copy-start.5 = (f32[2,128,2]{1,2,0:T(2,128)S(1)}, f32[2,128,2]{1,2,0:T(2,128)}, u32[]{:S(2)}) copy-start(f32[2,128,2]{1,2,0:T(2,128)} %param.13) | copy-start | bytes 6148
  31.2 42.5 %copy-start = (bf16[128,2048]{1,0:T(8,128)(2,1)S(1)}, bf16[128,2048]{1,0:T(8,128)(2,1)}, u32[]{:S(2)}) copy-start(bf16[128,2048]{1,0:T(8,128)(2,1)} %hid_ref.1) | copy-start | bytes 1572868

commit v8 on v7

--- a/solution.py
+++ b/solution.py
@@ -12,7 +12,7 @@
 SUB = 4
 CMP = 32
 KV = ("kv_0", "kv_1", "kv_2")
-GROUP_AXES = KV[1:]
+GROUP_AXES = (KV[2], KV[1])
 FAR = 1 << 30
 WIDE = jnp.float32
 LOW = jnp.bfloat16
@@ -31,6 +31,10 @@
 LAST = ROWS + 8 + COLS
 
 
+def slot(at):
+    return (at & 7) * NEAR + (at >> 3)
+
+
 def dot(a, b, ca, cb):
     return lax.dot_general(a, b, (((ca,), (cb,)), ((), ())), preferred_element_type=WIDE)
 
@@ -55,11 +59,12 @@
     means = jnp.mean(rows, 1).astype(LOW)
 
     def one(g, carry):
-        out_ref[g, SUMS:, :] = means
+        to = slot(g)
+        out_ref[to, SUMS:, :] = means
         for z in range(SLOW):
             pick = jnp.minimum(table_ref[z, column + g], PER - 1)
             at = pl.multiple_of((z * PER + pick) * BLK, BLK)
-            out_ref[g, z * BLK:(z + 1) * BLK, :] = all_ref[pl.ds(at, BLK), :]
+            out_ref[to, z * BLK:(z + 1) * BLK, :] = all_ref[pl.ds(at, BLK), :]
         return carry
 
     lax.fori_loop(0, GROUP, one, 0, unroll=2)
@@ -96,6 +101,9 @@
 def main_kernel(place_ref, list_ref, msum_ref, msel_ref, ldsum_ref, ldsel_ref, arr_ref, hid_ref,
                 dq_ref, ret_ref, kv_ref):
     base = place_ref[0] * ROWS
+    after = jnp.minimum(place_ref[0] + 1, SLOW * GROUP - 1)
+    spare = slot(after & (GROUP - 1))
+    spare_at = after // GROUP * BLK
     scale = DH ** (-0.5)
 
     def grads(m, kv, seen, ld):
@@ -115,7 +123,8 @@
     dq_sum = jnp.zeros((2 * ROWS, PAIR), WIDE)
     for y in range(0, GROUP, step):
         kv = jnp.concatenate([arr_ref[y + k, SUMS:, :] for k in range(step)], 0)
-        owner = (lane & (per_one - 1)) // PER * GROUP + y + lane // per_one
+        group = y + lane // per_one
+        owner = (lane & (per_one - 1)) // PER * GROUP + (group & (NEAR - 1)) * 8 + group // NEAR
         ends = (owner * PER + (lane & (PER - 1)) + 1) * CMP - 1 - base
         dq_part, kv_grad = grads(m, kv, ends <= row_at, ld)
         dq_sum += dq_part
@@ -131,22 +140,21 @@
             n = list_ref[0, s * TOPN + i]
             live = n >= 0
             owner = jnp.maximum(n, 0) // PER
-            fast = owner & (GROUP - 1)
+            fast = slot(owner & (GROUP - 1))
             at = pl.multiple_of(owner // GROUP * BLK, BLK)
             places.append((live, fast, at))
-            kv_ref[i * BLK:(i + 1) * BLK, :] = arr_ref[fast, pl.ds(at, BLK), :]
+            kv_ref[s, i * BLK:(i + 1) * BLK, :] = arr_ref[fast, pl.ds(at, BLK), :]
             start = jnp.where(live, n * BLK - base - i * BLK, FAR)
             at_key = jnp.where(sel_lane // BLK == i, start, at_key)
-        kv = kv_ref[...]
+        kv = kv_ref[s]
         seen = at_key + sel_lane <= sub_at + s * SUB_ROWS
         dq_part, kv_grad = grads(msel_ref[s], kv, seen, ldsel_ref[s])
         low = kv_grad.astype(LOW)
         for i in range(TOPN):
             live, fast, at = places[i]
-
-            @pl.when(live)
-            def _(fast=fast, at=at, i=i):
-                ret_ref[fast, pl.ds(at, BLK), :] = low[i * BLK:(i + 1) * BLK]
+            fast = jnp.where(live, fast, spare)
+            at = jnp.where(live, at, spare_at)
+            ret_ref[fast, pl.ds(pl.multiple_of(at, BLK), BLK), :] = low[i * BLK:(i + 1) * BLK]
 
         top = s * SUB_ROWS
         for h in range(2):
@@ -158,7 +166,7 @@
     for z in range(SLOW):
         part = dot(hid_ref[:, z * span:(z + 1) * span], qb, 0, 0).astype(LOW)
         for y in range(GROUP):
-            ret_ref[y, PARTS + z * COLS:PARTS + (z + 1) * COLS, :] = part[y * COLS:(y + 1) * COLS]
+            ret_ref[slot(y), PARTS + z * COLS:PARTS + (z + 1) * COLS, :] = part[y * COLS:(y + 1) * COLS]
 
 
 def merge_kernel(place_ref, table_ref, in_ref, out_ref, tail_ref):
@@ -175,10 +183,11 @@
 
         def one(g, carry, z=z):
             sums, cols = carry
+            here_at = slot(g)
             pick = table_ref[z, column + g]
-            here = in_ref[g, z * BLK:(z + 1) * BLK, :].astype(WIDE)
+            here = in_ref[here_at, z * BLK:(z + 1) * BLK, :].astype(WIDE)
             sums = tuple(sums[b] + jnp.where(pick == b, here, 0.0) for b in range(PER))
-            part = in_ref[g, PARTS + z * COLS:PARTS + (z + 1) * COLS, :]
+            part = in_ref[here_at, PARTS + z * COLS:PARTS + (z + 1) * COLS, :]
             return sums, cols + part.astype(WIDE)
 
         zero = jnp.zeros((BLK, PAIR), WIDE)
@@ -269,7 +278,7 @@
         main_kernel,
         [smem(), smem()] + [vmem()] * 6,
         (shape(ROWS, PAIR, kind=WIDE), local(GROUP, BACK, PAIR)),
-        (pltpu.VMEM((TOPN * BLK, PAIR), LOW),),
+        (pltpu.VMEM((SUB, TOPN * BLK, PAIR), LOW),),
     )(here, listing, *inside(m_sum, m_sel, ld_sum, ld_sel, arrived, hidden))
     across = lax.all_to_all(returned, GROUP_AXES, split_axis=0, concat_axis=0, tiled=True)
     merged = call(

time: 148 us -> 147 us (level)
    all_to_all x1, blocking collectives: 22.5 us -> 19.8 us  [shards(): lax.all_to_all(merged, KV[0], split_axis=0, concat_axis=0, tiled=True)]
where the time goes in v8:
time: 147 us; the launch traced here: 146 us
  blocking collectives  137 us (93%)
  Pallas kernels  8.21 us (6%)
    all_to_all x1, blocking collectives, shards(): lax.all_to_all(returned, GROUP_AXES, split_axis=0, concat_axis=0, tiled=T...  45.3 us
    all_to_all x1, blocking collectives, shards(): lax.all_to_all(outbound, GROUP_AXES, split_axis=0, concat_axis=0, tiled=T...  42.1 us
    all_gather x1, blocking collectives, shards(): along = lax.all_gather(pairs, KV[0], axis=0, tiled=True)  29.7 us
    all_to_all x1, blocking collectives, shards(): lax.all_to_all(merged, KV[0], split_axis=0, concat_axis=0, tiled=True)  19.8 us
    pallas_call x1, Pallas kernels, shards(): call(main_kernel, [smem(), smem()] + [vmem()] * 6, (shape(ROWS, PAIR, kin...  3.26 us

profile of v8, /device:TPU:6, one launch (start us, length us, event | category | flops | bytes accessed | tf_op | source)
XLA Modules:
  0.0 145.8 jit_solution(10979114558714098472)
XLA Ops:
  0.6 0.9 pairs_kernel.1
  1.5 29.7 %all_gather.3.all_ref = bf16[512,128]{1,0:T(8,128)(2,1)S(1)} all-gather(bf16[128,128]{1,0:T(8,128)(2,1)S(1)} %get-tuple-element.20), channel_id=1, replica_groups=mesh['kv_0'=4,'kv_1'=4,'kv_2'=8,'tp'=8] {'kv_0'}, dimensions={0}, use_global_device_ids=true | all-gather | bytes 163840 | tf_op jit(solution)/shard_map/all_gather | solution.py:262
  31.2 0.0 copy-start.1
  31.2 0.0 copy-start.2
  31.2 0.0 copy-start.3
  31.2 0.0 copy-start.4
  31.2 0.0 copy-start.5
  31.2 0.0 copy-start
  31.2 1.1 relay_kernel.1
  32.3 42.1 %all_to_all.15.arr_ref = bf16[32,144,128]{2,1,0:T(8,128)(2,1)S(1)} all-to-all(bf16[32,144,128]{2,1,0:T(8,128)(2,1)S(1)} %relay_kernel.1), channel_id=1, replica_groups=mesh['kv_0'=4,'kv_1'=4,'kv_2'=8,'tp'=8] {'kv_2','kv_1'}, dimensions={0} | all-to-all | bytes 2359296 | tf_op jit(solution)/shard_map/all_to_all | solution.py:264
  74.4 0.0 copy-done.1
  74.4 0.0 copy-done.2
  74.4 0.0 copy-done.3
  74.4 0.0 copy-done.4
  74.4 0.0 copy-done.5
  74.4 0.6 prep_kernel.1
  75.0 0.0 copy-done
  75.0 3.3 %main_kernel.1 = (f32[128,128]{1,0:T(8,128)}, bf16[32,208,128]{2,1,0:T(8,128)(2,1)S(1)}) custom-call(s32[1]{0:T(128)} %bitcast.place_ref, s32[1,48]{1,0:T(1,128)S(1)} %get-tuple-element.18.list_ref, bf16[512,128]{1,0:T(8,128)(2,1)S(1)} %get-tuple-element.22.msum_ref, bf16[4,128,128]{2,1,0:T(8,128)(2,1)S(1)} %get-tuple-element.23.msel_ref, ...), custom_call_target="tpu_custom_call" | custom-call | tf_op jit(solution)/shard_map/main_kernel/pallas_call | solution.py:277
  78.3 45.3 %all_to_all.16.in_ref = bf16[32,208,128]{2,1,0:T(8,128)(2,1)S(1)} all-to-all(bf16[32,208,128]{2,1,0:T(8,128)(2,1)S(1)} %get-tuple-element.28), channel_id=1, replica_groups=mesh['kv_0'=4,'kv_1'=4,'kv_2'=8,'tp'=8] {'kv_2','kv_1'}, dimensions={0} | all-to-all | bytes 3407872 | tf_op jit(solution)/shard_map/all_to_all | solution.py:283
  123.6 1.7 %merge_kernel.1 = bf16[4,152,128]{2,1,0:T(8,128)(2,1)S(1)} custom-call(s32[1]{0:T(128)} %bitcast.place_ref, s32[4,128]{1,0:T(4,128)S(1)} %get-tuple-element.19.table_ref, bf16[32,208,128]{2,1,0:T(8,128)(2,1)S(1)} %all_to_all.16.in_ref), custom_call_target="tpu_custom_call" | custom-call | tf_op jit(solution)/shard_map/merge_kernel/pallas_call | solution.py:284
  125.2 19.8 %all_to_all.17.in_ref = bf16[4,152,128]{2,1,0:T(8,128)(2,1)S(1)} all-to-all(bf16[4,152,128]{2,1,0:T(8,128)(2,1)S(1)} %merge_kernel.1), channel_id=1, replica_groups=mesh['kv_0'=4,'kv_1'=4,'kv_2'=8,'tp'=8] {'kv_0'}, dimensions={0} | all-to-all | bytes 311296 | tf_op jit(solution)/shard_map/all_to_all | solution.py:290
  145.1 0.7 final_kernel.1
Async XLA Ops:
  31.2 43.2 %copy-start.1 = (bf16[2,128,128]{2,1,0:T(8,128)(2,1)S(1)}, bf16[2,128,128]{2,1,0:T(8,128)(2,1)}, u32[]{:S(2)}) copy-start(bf16[2,128,128]{2,1,0:T(8,128)(2,1)} %out_ref.1) | copy-start | bytes 196612
  31.2 43.2 %copy-start.2 = (bf16[128,128]{1,0:T(8,128)(2,1)S(1)}, bf16[128,128]{1,0:T(8,128)(2,1)}, u32[]{:S(2)}) copy-start(bf16[128,128]{1,0:T(8,128)(2,1)} %q_ref) | copy-start | bytes 98308
  31.2 43.2 %copy-start.3 = (bf16[128,128]{1,0:T(8,128)(2,1)S(1)}, bf16[128,128]{1,0:T(8,128)(2,1)}, u32[]{:S(2)}) copy-start(bf16[128,128]{1,0:T(8,128)(2,1)} %cot_ref.1) | copy-start | bytes 98308
  31.2 43.2 %copy-start.4 = (f32[2,128,2]{1,2,0:T(2,128)S(1)}, f32[2,128,2]{1,2,0:T(2,128)}, u32[]{:S(2)}) copy-start(f32[2,128,2]{1,2,0:T(2,128)} %param.14) | copy-start | bytes 6148
  31.2 43.2 %copy-start.5 = (f32[2,128,2]{1,2,0:T(2,128)S(1)}, f32[2,128,2]{1,2,0:T(2,128)}, u32[]{:S(2)}) copy-start(f32[2,128,2]{1,2,0:T(2,128)} %param.13) | copy-start | bytes 6148
  31.2 43.8 %copy-start = (bf16[128,2048]{1,0:T(8,128)(2,1)S(1)}, bf16[128,2048]{1,0:T(8,128)(2,1)}, u32[]{:S(2)}) copy-start(bf16[128,2048]{1,0:T(8,128)(2,1)} %hid_ref.1) | copy-start | bytes 1572868

commit v9 on v7

--- a/solution.py
+++ b/solution.py
@@ -96,6 +96,9 @@
 def main_kernel(place_ref, list_ref, msum_ref, msel_ref, ldsum_ref, ldsel_ref, arr_ref, hid_ref,
                 dq_ref, ret_ref, kv_ref):
     base = place_ref[0] * ROWS
+    after = jnp.minimum(place_ref[0] + 1, SLOW * GROUP - 1)
+    spare = after & (GROUP - 1)
+    spare_at = after // GROUP * BLK
     scale = DH ** (-0.5)
 
     def grads(m, kv, seen, ld):
@@ -134,19 +137,18 @@
             fast = owner & (GROUP - 1)
             at = pl.multiple_of(owner // GROUP * BLK, BLK)
             places.append((live, fast, at))
-            kv_ref[i * BLK:(i + 1) * BLK, :] = arr_ref[fast, pl.ds(at, BLK), :]
+            kv_ref[s, i * BLK:(i + 1) * BLK, :] = arr_ref[fast, pl.ds(at, BLK), :]
             start = jnp.where(live, n * BLK - base - i * BLK, FAR)
             at_key = jnp.where(sel_lane // BLK == i, start, at_key)
-        kv = kv_ref[...]
+        kv = kv_ref[s]
         seen = at_key + sel_lane <= sub_at + s * SUB_ROWS
         dq_part, kv_grad = grads(msel_ref[s], kv, seen, ldsel_ref[s])
         low = kv_grad.astype(LOW)
         for i in range(TOPN):
             live, fast, at = places[i]
-
-            @pl.when(live)
-            def _(fast=fast, at=at, i=i):
-                ret_ref[fast, pl.ds(at, BLK), :] = low[i * BLK:(i + 1) * BLK]
+            fast = jnp.where(live, fast, spare)
+            at = jnp.where(live, at, spare_at)
+            ret_ref[fast, pl.ds(pl.multiple_of(at, BLK), BLK), :] = low[i * BLK:(i + 1) * BLK]
 
         top = s * SUB_ROWS
         for h in range(2):
@@ -269,7 +271,7 @@
         main_kernel,
         [smem(), smem()] + [vmem()] * 6,
         (shape(ROWS, PAIR, kind=WIDE), local(GROUP, BACK, PAIR)),
-        (pltpu.VMEM((TOPN * BLK, PAIR), LOW),),
+        (pltpu.VMEM((SUB, TOPN * BLK, PAIR), LOW),),
     )(here, listing, *inside(m_sum, m_sel, ld_sum, ld_sel, arrived, hidden))
     across = lax.all_to_all(returned, GROUP_AXES, split_axis=0, concat_axis=0, tiled=True)
     merged = call(

time: 148 us -> 147 us (level)
  no operation moved by 1% of the time
where the time goes in v9:
time: 147 us
  blocking collectives  138 us (94%)
  Pallas kernels  8.03 us (5%)
    all_to_all x1, blocking collectives, shards(): lax.all_to_all(returned, GROUP_AXES, split_axis=0, concat_axis=0, tiled=T...  44.8 us
    all_to_all x1, blocking collectives, shards(): lax.all_to_all(outbound, GROUP_AXES, split_axis=0, concat_axis=0, tiled=T...  40.8 us
    all_gather x1, blocking collectives, shards(): along = lax.all_gather(pairs, KV[0], axis=0, tiled=True)  29.7 us
    all_to_all x1, blocking collectives, shards(): lax.all_to_all(merged, KV[0], split_axis=0, concat_axis=0, tiled=True)  22.4 us
    pallas_call x1, Pallas kernels, shards(): call(main_kernel, [smem(), smem()] + [vmem()] * 6, (shape(ROWS, PAIR, kin...  3.23 us

profile of v9, /device:TPU:6, one launch (start us, length us, event | category | flops | bytes accessed | tf_op | source)
XLA Modules:
  0.0 146.5 jit_solution(13545814684659714380)
XLA Ops:
  0.6 0.9 pairs_kernel.1
  1.5 29.7 %all_gather.3.all_ref = bf16[512,128]{1,0:T(8,128)(2,1)S(1)} all-gather(bf16[128,128]{1,0:T(8,128)(2,1)S(1)} %get-tuple-element.20), channel_id=1, replica_groups=mesh['kv_0'=4,'kv_1'=4,'kv_2'=8,'tp'=8] {'kv_0'}, dimensions={0}, use_global_device_ids=true | all-gather | bytes 163840 | tf_op jit(solution)/shard_map/all_gather | solution.py:255
  31.2 0.0 copy-start.1
  31.2 0.0 copy-start.2
  31.2 0.0 copy-start.3
  31.2 0.0 copy-start.4
  31.2 0.0 copy-start.5
  31.2 0.0 copy-start
  31.2 1.0 relay_kernel.1
  32.3 40.8 %all_to_all.15.arr_ref = bf16[32,144,128]{2,1,0:T(8,128)(2,1)S(1)} all-to-all(bf16[32,144,128]{2,1,0:T(8,128)(2,1)S(1)} %relay_kernel.1), channel_id=1, replica_groups=mesh['kv_0'=4,'kv_1'=4,'kv_2'=8,'tp'=8] {'kv_1','kv_2'}, dimensions={0} | all-to-all | bytes 2359296 | tf_op jit(solution)/shard_map/all_to_all | solution.py:257
  73.1 0.0 copy-done.1
  73.1 0.0 copy-done.2
  73.1 0.0 copy-done.3
  73.1 0.0 copy-done.4
  73.1 0.0 copy-done.5
  73.1 0.6 prep_kernel.1
  73.7 0.0 copy-done
  73.7 3.2 %main_kernel.1 = (f32[128,128]{1,0:T(8,128)}, bf16[32,208,128]{2,1,0:T(8,128)(2,1)S(1)}) custom-call(s32[1]{0:T(128)} %bitcast.place_ref, s32[1,48]{1,0:T(1,128)S(1)} %get-tuple-element.18.list_ref, bf16[512,128]{1,0:T(8,128)(2,1)S(1)} %get-tuple-element.22.msum_ref, bf16[4,128,128]{2,1,0:T(8,128)(2,1)S(1)} %get-tuple-element.23.msel_ref, ...), custom_call_target="tpu_custom_call" | custom-call | tf_op jit(solution)/shard_map/main_kernel/pallas_call | solution.py:270
  77.0 44.8 %all_to_all.16.in_ref = bf16[32,208,128]{2,1,0:T(8,128)(2,1)S(1)} all-to-all(bf16[32,208,128]{2,1,0:T(8,128)(2,1)S(1)} %get-tuple-element.28), channel_id=1, replica_groups=mesh['kv_0'=4,'kv_1'=4,'kv_2'=8,'tp'=8] {'kv_1','kv_2'}, dimensions={0} | all-to-all | bytes 3407872 | tf_op jit(solution)/shard_map/all_to_all | solution.py:276
  121.8 1.6 %merge_kernel.1 = bf16[4,152,128]{2,1,0:T(8,128)(2,1)S(1)} custom-call(s32[1]{0:T(128)} %bitcast.place_ref, s32[4,128]{1,0:T(4,128)S(1)} %get-tuple-element.19.table_ref, bf16[32,208,128]{2,1,0:T(8,128)(2,1)S(1)} %all_to_all.16.in_ref), custom_call_target="tpu_custom_call" | custom-call | tf_op jit(solution)/shard_map/merge_kernel/pallas_call | solution.py:277
  123.4 22.4 %all_to_all.17.in_ref = bf16[4,152,128]{2,1,0:T(8,128)(2,1)S(1)} all-to-all(bf16[4,152,128]{2,1,0:T(8,128)(2,1)S(1)} %merge_kernel.1), channel_id=1, replica_groups=mesh['kv_0'=4,'kv_1'=4,'kv_2'=8,'tp'=8] {'kv_0'}, dimensions={0} | all-to-all | bytes 311296 | tf_op jit(solution)/shard_map/all_to_all | solution.py:283
  145.8 0.7 final_kernel.1
Async XLA Ops:
  31.2 41.9 %copy-start.1 = (bf16[2,128,128]{2,1,0:T(8,128)(2,1)S(1)}, bf16[2,128,128]{2,1,0:T(8,128)(2,1)}, u32[]{:S(2)}) copy-start(bf16[2,128,128]{2,1,0:T(8,128)(2,1)} %out_ref.1) | copy-start | bytes 196612
  31.2 41.9 %copy-start.2 = (bf16[128,128]{1,0:T(8,128)(2,1)S(1)}, bf16[128,128]{1,0:T(8,128)(2,1)}, u32[]{:S(2)}) copy-start(bf16[128,128]{1,0:T(8,128)(2,1)} %q_ref) | copy-start | bytes 98308
  31.2 41.9 %copy-start.3 = (bf16[128,128]{1,0:T(8,128)(2,1)S(1)}, bf16[128,128]{1,0:T(8,128)(2,1)}, u32[]{:S(2)}) copy-start(bf16[128,128]{1,0:T(8,128)(2,1)} %cot_ref.1) | copy-start | bytes 98308
  31.2 41.9 %copy-start.4 = (f32[2,128,2]{1,2,0:T(2,128)S(1)}, f32[2,128,2]{1,2,0:T(2,128)}, u32[]{:S(2)}) copy-start(f32[2,128,2]{1,2,0:T(2,128)} %param.14) | copy-start | bytes 6148
  31.2 41.9 %copy-start.5 = (f32[2,128,2]{1,2,0:T(2,128)S(1)}, f32[2,128,2]{1,2,0:T(2,128)}, u32[]{:S(2)}) copy-start(f32[2,128,2]{1,2,0:T(2,128)} %param.13) | copy-start | bytes 6148
  31.2 42.5 %copy-start = (bf16[128,2048]{1,0:T(8,128)(2,1)S(1)}, bf16[128,2048]{1,0:T(8,128)(2,1)}, u32[]{:S(2)}) copy-start(bf16[128,2048]{1,0:T(8,128)(2,1)} %hid_ref.1) | copy-start | bytes 1572868

commit v10 on v9

--- a/solution.py
+++ b/solution.py
@@ -37,7 +37,7 @@
 
 def pairs_kernel(place_ref, keys_ref, values_ref, chosen_ref, out_ref, table_ref, list_ref, turned_ref):
     both = jnp.concatenate([keys_ref[...], values_ref[...]], 0).astype(WIDE)
-    out_ref[...] = both.T.astype(LOW)
+    out_ref[...] = both.T.reshape(PER, BLK, PAIR).astype(LOW)
     entry = chosen_ref[...]
     turned_ref[...] = entry.T
     list_ref[...] = turned_ref[pl.ds(place_ref[0], 1), :]
@@ -51,15 +51,14 @@
 
 def relay_kernel(place_ref, table_ref, all_ref, out_ref):
     column = place_ref[0] // GROUP * GROUP
-    rows = all_ref[...].astype(WIDE).reshape(SLOW * PER, CMP, PAIR)
+    rows = all_ref[...].astype(WIDE)
     means = jnp.mean(rows, 1).astype(LOW)
 
     def one(g, carry):
         out_ref[g, SUMS:, :] = means
         for z in range(SLOW):
             pick = jnp.minimum(table_ref[z, column + g], PER - 1)
-            at = pl.multiple_of((z * PER + pick) * BLK, BLK)
-            out_ref[g, z * BLK:(z + 1) * BLK, :] = all_ref[pl.ds(at, BLK), :]
+            out_ref[g, z * BLK:(z + 1) * BLK, :] = all_ref[z * PER + pick]
         return carry
 
     lax.fori_loop(0, GROUP, one, 0, unroll=2)
@@ -246,7 +245,7 @@
         pairs_kernel,
         [smem(), vmem(), vmem(), vmem()],
         (
-            local(ROWS, PAIR),
+            local(PER, BLK, PAIR),
             shape(SLOW, lists.shape[0], kind=jnp.int32),
             shape(1, lists.shape[1], kind=jnp.int32),
         ),

time: 147 us -> 147 us (level)
  no operation moved by 1% of the time
where the time goes in v10:
time: 147 us; the launch traced here: 146 us
  blocking collectives  138 us (94%)
  Pallas kernels  7.94 us (5%)
    all_to_all x1, blocking collectives, shards(): lax.all_to_all(returned, GROUP_AXES, split_axis=0, concat_axis=0, tiled=T...  44.8 us
    all_to_all x1, blocking collectives, shards(): lax.all_to_all(outbound, GROUP_AXES, split_axis=0, concat_axis=0, tiled=T...  40.8 us
    all_gather x1, blocking collectives, shards(): along = lax.all_gather(pairs, KV[0], axis=0, tiled=True)  29.7 us
    all_to_all x1, blocking collectives, shards(): lax.all_to_all(merged, KV[0], split_axis=0, concat_axis=0, tiled=True)  22.4 us
    pallas_call x1, Pallas kernels, shards(): call(main_kernel, [smem(), smem()] + [vmem()] * 6, (shape(ROWS, PAIR, kin...  3.23 us

profile of v10, /device:TPU:6, one launch (start us, length us, event | category | flops | bytes accessed | tf_op | source)
XLA Modules:
  0.0 146.4 jit_solution(15044669121036993150)
XLA Ops:
  0.6 0.9 pairs_kernel.1
  1.5 29.7 %all_gather.3.all_ref = bf16[16,32,128]{2,1,0:T(8,128)(2,1)S(1)} all-gather(bf16[4,32,128]{2,1,0:T(8,128)(2,1)S(1)} %get-tuple-element.20), channel_id=1, replica_groups=mesh['kv_0'=4,'kv_1'=4,'kv_2'=8,'tp'=8] {'kv_0'}, dimensions={0}, use_global_device_ids=true | all-gather | bytes 163840 | tf_op jit(solution)/shard_map/all_gather | solution.py:254
  31.2 0.0 copy-start.1
  31.2 0.0 copy-start.2
  31.2 0.0 copy-start.3
  31.2 0.0 copy-start.4
  31.2 0.0 copy-start.5
  31.2 0.0 copy-start
  31.2 0.9 relay_kernel.1
  32.2 40.8 %all_to_all.15.arr_ref = bf16[32,144,128]{2,1,0:T(8,128)(2,1)S(1)} all-to-all(bf16[32,144,128]{2,1,0:T(8,128)(2,1)S(1)} %relay_kernel.1), channel_id=1, replica_groups=mesh['kv_0'=4,'kv_1'=4,'kv_2'=8,'tp'=8] {'kv_1','kv_2'}, dimensions={0} | all-to-all | bytes 2359296 | tf_op jit(solution)/shard_map/all_to_all | solution.py:256
  73.0 0.0 copy-done.1
  73.0 0.0 copy-done.2
  73.0 0.0 copy-done.3
  73.0 0.0 copy-done.4
  73.0 0.0 copy-done.5
  73.0 0.6 prep_kernel.1
  73.6 0.0 copy-done
  73.6 3.2 %main_kernel.1 = (f32[128,128]{1,0:T(8,128)}, bf16[32,208,128]{2,1,0:T(8,128)(2,1)S(1)}) custom-call(s32[1]{0:T(128)} %bitcast.place_ref, s32[1,48]{1,0:T(1,128)S(1)} %get-tuple-element.18.list_ref, bf16[512,128]{1,0:T(8,128)(2,1)S(1)} %get-tuple-element.22.msum_ref, bf16[4,128,128]{2,1,0:T(8,128)(2,1)S(1)} %get-tuple-element.23.msel_ref, ...), custom_call_target="tpu_custom_call" | custom-call | tf_op jit(solution)/shard_map/main_kernel/pallas_call | solution.py:269
  76.9 44.8 %all_to_all.16.in_ref = bf16[32,208,128]{2,1,0:T(8,128)(2,1)S(1)} all-to-all(bf16[32,208,128]{2,1,0:T(8,128)(2,1)S(1)} %get-tuple-element.28), channel_id=1, replica_groups=mesh['kv_0'=4,'kv_1'=4,'kv_2'=8,'tp'=8] {'kv_1','kv_2'}, dimensions={0} | all-to-all | bytes 3407872 | tf_op jit(solution)/shard_map/all_to_all | solution.py:275
  121.7 1.6 %merge_kernel.1 = bf16[4,152,128]{2,1,0:T(8,128)(2,1)S(1)} custom-call(s32[1]{0:T(128)} %bitcast.place_ref, s32[4,128]{1,0:T(4,128)S(1)} %get-tuple-element.19.table_ref, bf16[32,208,128]{2,1,0:T(8,128)(2,1)S(1)} %all_to_all.16.in_ref), custom_call_target="tpu_custom_call" | custom-call | tf_op jit(solution)/shard_map/merge_kernel/pallas_call | solution.py:276
  123.3 22.4 %all_to_all.17.in_ref = bf16[4,152,128]{2,1,0:T(8,128)(2,1)S(1)} all-to-all(bf16[4,152,128]{2,1,0:T(8,128)(2,1)S(1)} %merge_kernel.1), channel_id=1, replica_groups=mesh['kv_0'=4,'kv_1'=4,'kv_2'=8,'tp'=8] {'kv_0'}, dimensions={0} | all-to-all | bytes 311296 | tf_op jit(solution)/shard_map/all_to_all | solution.py:282
  145.7 0.7 final_kernel.1
Async XLA Ops:
  31.2 41.8 %copy-start.1 = (bf16[2,128,128]{2,1,0:T(8,128)(2,1)S(1)}, bf16[2,128,128]{2,1,0:T(8,128)(2,1)}, u32[]{:S(2)}) copy-start(bf16[2,128,128]{2,1,0:T(8,128)(2,1)} %out_ref.1) | copy-start | bytes 196612
  31.2 41.8 %copy-start.2 = (bf16[128,128]{1,0:T(8,128)(2,1)S(1)}, bf16[128,128]{1,0:T(8,128)(2,1)}, u32[]{:S(2)}) copy-start(bf16[128,128]{1,0:T(8,128)(2,1)} %q_ref) | copy-start | bytes 98308
  31.2 41.8 %copy-start.3 = (bf16[128,128]{1,0:T(8,128)(2,1)S(1)}, bf16[128,128]{1,0:T(8,128)(2,1)}, u32[]{:S(2)}) copy-start(bf16[128,128]{1,0:T(8,128)(2,1)} %cot_ref.1) | copy-start | bytes 98308
  31.2 41.8 %copy-start.4 = (f32[2,128,2]{1,2,0:T(2,128)S(1)}, f32[2,128,2]{1,2,0:T(2,128)}, u32[]{:S(2)}) copy-start(f32[2,128,2]{1,2,0:T(2,128)} %param.14) | copy-start | bytes 6148
  31.2 41.8 %copy-start.5 = (f32[2,128,2]{1,2,0:T(2,128)S(1)}, f32[2,128,2]{1,2,0:T(2,128)}, u32[]{:S(2)}) copy-start(f32[2,128,2]{1,2,0:T(2,128)} %param.13) | copy-start | bytes 6148
  31.2 42.4 %copy-start = (bf16[128,2048]{1,0:T(8,128)(2,1)S(1)}, bf16[128,2048]{1,0:T(8,128)(2,1)}, u32[]{:S(2)}) copy-start(bf16[128,2048]{1,0:T(8,128)(2,1)} %hid_ref.1) | copy-start | bytes 1572868
